TPU v7x, 128 devices: a whole 4x4x4 slice. The times are simulated.
128 devices in a mesh: sp: 16 (over z, x), tp: 8 (over y, core).
Axes of the slice: x: 4, y: 4, z: 4, core: 2. Of those that a mesh axis runs over, the one named last changes fastest.
Arguments:
- resid: bfloat16 [12288, 3072], P('sp', 'tp'), may hold values from -12 to 12
- query: bfloat16 [12288, 1536], P('sp', 'tp'), may hold values from -6 to 6
- keys: bfloat16 [12288, 1536], P('sp', 'tp'), may hold values from -6 to 6
- values: bfloat16 [12288, 1536], P('sp', 'tp'), may hold values from -6 to 6
- out_gate: bfloat16 [12288, 1536], P('sp', 'tp'), may hold values from -6 to 6
- in_gate: float32 [16, 12288], P('tp', 'sp'), may hold values from -6 to 110
- forget: float32 [16, 12288], P('tp', 'sp'), may hold values from -1 to 16
- doc_ids: int32 [12288], P('sp'), may hold values from 0 to 7, never falling along the last dimension, each value on 1 to 3072 neighbouring positions
- head_gain: float32 [1536], P('tp'), may hold values from 0.1 to 1.9
- w_out: bfloat16 [1536, 3072], P('tp'), may hold values from -0.15625 to 0.15625
- ffn_gain: float32 [3072], replicated, may hold values from 0.1 to 1.9
- w_gate: bfloat16 [3072, 8448], P('sp', 'tp'), may hold values from -0.109375 to 0.109375
- w_value: bfloat16 [3072, 8448], P('sp', 'tp'), may hold values from -0.109375 to 0.109375
- conv_taps: float32 [3, 8448], P(None, 'tp'), may hold values from -3.5 to 3.5
- w_down: bfloat16 [8448, 3072], P('tp', 'sp'), may hold values from -0.0625 to 0.0625
Outputs:
- layer_out: bfloat16 [12288, 3072], P('sp', 'tp')
Inputs may be any that keep to these rules, and one draw needn't show every extreme that they name: `doc_ids`: document numbers never fall along the positions; each document is 1 to 3072 positions long.
All inputs are finite; a program needn't handle non-finite values.
Results may differ from a plain program's by a relative error of at most 0.02.
Values may be sent and summed in bfloat16 or wider, within the bound.
A program may use at most 128 MiB of HBM per device.

v0:
```python
import jax
import jax.numpy as jnp
from jax import lax
from jax.sharding import Mesh
from jax.sharding import PartitionSpec as P

DH = 96
BLOCK = 64
SP = ("sp_0", "sp_1")


ABSENT = -1e30
epsilon = 1e-06
head_floor = 1.0


def nothing_yet(value, identity):
    return jax.tree.map(
        lambda part, zero: jnp.zeros_like(part) + jnp.asarray(zero, part.dtype), value, identity
    )


def collected_together(value, axis):
    leaves = jax.tree.leaves(value)
    order = sorted(range(len(leaves)), key=lambda k: -leaves[k].size)
    width = (1, *leaves[order[0]].shape)[-1]
    lines = [
        jnp.pad(leaves[k].reshape(-1), (0, -leaves[k].size % width)).reshape(-1, width)
        for k in order
    ]
    both, at, found = (lax.all_gather(jnp.concatenate(lines), axis), 0, {})
    for k, line in zip(order, lines):
        share = both[:, at : at + len(line)].reshape(len(both), -1)
        found[k] = share[:, : leaves[k].size].reshape(-1, *leaves[k].shape)
        at += len(line)
    numbers = iter(range(len(leaves)))
    return jax.tree.map(lambda _: found[next(numbers)], value)


def prefix_by_axis(value, axes, combine, identity):
    before = start = nothing_yet(value, identity)
    subtotal = value
    for axis in reversed(axes):
        length, index = (lax.axis_size(axis), lax.axis_index(axis))
        pieces = collected_together(subtotal, axis)
        inside, subtotal = (start, start)
        for k in range(length):
            passed = k < index
            subtotal = combine(subtotal, jax.tree.map(lambda part: part[k], pieces))
            inside = jax.tree.map(lambda new, old: jnp.where(passed, new, old), subtotal, inside)
        before = combine(inside, before)
    return before


def in_one_piece(arrays, axis, dim, along):
    widths = [a.shape[along] for a in arrays]
    both = jnp.concatenate(arrays, axis=along)
    result = lax.all_gather(both, axis, axis=dim, tiled=True)
    return tuple(jnp.split(result, [sum(widths[:k]) for k in range(1, len(widths))], axis=along))


def passed_along(value, axis, steps):
    count = lax.axis_size(axis)
    initial, last = (max(0, -steps), min(count, count - steps))
    return lax.ppermute(value, axis, [(source, source + steps) for source in range(initial, last)])


def combine(early, late):
    state_early, peak_early, decay_early, first_early, last_early, second_early = early
    state_late, peak_late, decay_late, first_late, last_late, second_late = late
    early_empty = last_early < 0.0
    late_empty = first_late < 0.0
    cut = (first_late != last_early) & jnp.logical_not(early_empty) & jnp.logical_not(late_empty)
    passed = jnp.where(cut, ABSENT, decay_late)
    peak = jnp.maximum(passed + peak_early, peak_late)
    keep = jnp.exp(passed + peak_early - peak)
    fresh = jnp.exp(peak_late - peak)
    state = keep[..., None, None] * state_early + fresh[..., None, None] * state_late
    return (
        state,
        peak,
        decay_early + passed,
        jnp.where(early_empty, first_late, first_early),
        jnp.where(late_empty, last_early, last_late),
        jnp.where(late_empty, second_early, second_late),
    )


def empty_state(heads, width):
    return (
        jnp.zeros((heads, width, width), jnp.float32),
        jnp.full((heads,), ABSENT, jnp.float32),
        jnp.zeros((heads,), jnp.float32),
        jnp.full((1,), -1.0, jnp.float32),
        jnp.full((1,), -1.0, jnp.float32),
        jnp.full((1,), -1.0, jnp.float32),
    )


def advance(carry, item):
    return (combine(carry, item), carry)


def block_parts(query, keys, values, in_gate, forget, seg):
    length, heads, width = query.shape
    count = length // BLOCK
    query_blocks = query.reshape(count, BLOCK, heads, width)
    key_blocks = (keys * width ** (-0.5)).reshape(count, BLOCK, heads, width)
    value_blocks = values.reshape(count, BLOCK, heads, width)
    gate_in = in_gate.T.reshape(count, BLOCK, heads)
    cumul = jnp.cumsum(jax.nn.log_sigmoid(forget.T).reshape(count, BLOCK, heads), axis=1)
    seg_blocks = seg.reshape(count, BLOCK)
    total = cumul[:, -1]
    in_last = (seg_blocks == seg_blocks[:, -1:])[:, :, None]
    weight_log = jnp.where(in_last, total[:, None] - cumul + gate_in, ABSENT)
    local_peak = jnp.max(weight_log, axis=1)
    weights = jnp.exp(weight_log - local_peak[:, None])
    update = jnp.einsum("nchk,nchv->nhkv", weights[..., None] * key_blocks, value_blocks)
    whole = jnp.all(seg_blocks == seg_blocks[:, :1], axis=1)[:, None]
    decay = jnp.where(whole, total, ABSENT)
    elements = (
        update,
        local_peak,
        decay,
        seg_blocks[:, :1],
        seg_blocks[:, -1:],
        seg_blocks[:, -2:-1],
    )
    return (elements, (query_blocks, key_blocks, value_blocks, gate_in, cumul, seg_blocks))


def block_outputs(before, parts):
    state, peak_prev, _, _, last_prev, _ = before
    query_blocks, key_blocks, value_blocks, gate_in, cumul, seg_blocks = parts
    count, span, heads, width = query_blocks.shape
    carried = (seg_blocks == last_prev)[:, :, None]
    inter = jnp.where(carried, cumul + peak_prev[:, None], ABSENT)
    places = jnp.arange(span)
    causal = (places[:, None] >= places[None, :])[None, :, :, None]
    same = (seg_blocks[:, :, None] == seg_blocks[:, None, :])[..., None]
    diff_log = jnp.where(
        causal & same, cumul[:, :, None] - cumul[:, None] + gate_in[:, None], ABSENT
    )
    top = jnp.maximum(inter, jnp.max(diff_log, axis=2))
    scores = jnp.einsum("nthd,nshd->ntsh", query_blocks, key_blocks) * jnp.exp(
        diff_log - top[:, :, None]
    )
    result = jnp.einsum("ntsh,nshd->nthd", scores, value_blocks)
    result = result + jnp.exp(inter - top)[..., None] * jnp.einsum(
        "nthk,nhkv->nthv", query_blocks, state
    )
    return result.reshape(count * span, heads, width)


def body(
    resid,
    query,
    keys,
    values,
    out_gate,
    in_gate,
    forget,
    doc_ids,
    head_gain,
    w_out,
    ffn_gain,
    w_gate,
    w_value,
    conv_taps,
    w_down,
):
    tokens = query.shape[0]
    heads = query.shape[1] // DH
    seg = doc_ids.astype(jnp.float32)
    query_f = query.astype(jnp.float32).reshape(tokens, heads, DH)
    keys_f = keys.astype(jnp.float32).reshape(tokens, heads, DH)
    values_f = values.astype(jnp.float32).reshape(tokens, heads, DH)
    elements, parts = block_parts(query_f, keys_f, values_f, in_gate, forget, seg)
    local_end, before = lax.scan(advance, empty_state(heads, DH), elements)
    incoming = prefix_by_axis(local_end, SP, combine, empty_state(heads, DH))
    starts = combine(incoming, before)
    memory_out = block_outputs(starts, parts)
    normed = memory_out * lax.rsqrt(
        jnp.mean(memory_out * memory_out, axis=-1, keepdims=True) + head_floor
    )
    normed = (
        normed.reshape(tokens, heads * DH)
        * head_gain
        * jax.nn.sigmoid(out_gate.astype(jnp.float32))
    )
    mix = normed.astype(jnp.bfloat16)
    share = jnp.dot(mix, w_out, preferred_element_type=jnp.float32).astype(jnp.bfloat16)
    term = lax.optimization_barrier(share).astype(jnp.float32)
    local_cols = resid.shape[1]
    offset = lax.axis_index("tp") * local_cols
    placed = lax.dynamic_update_slice_in_dim(
        jnp.zeros_like(term), resid.astype(jnp.float32), offset, 1
    )
    full_rows = lax.psum(term + placed, "tp")
    scale = lax.rsqrt(jnp.mean(full_rows * full_rows, axis=1, keepdims=True) + epsilon)
    normed_rows = (full_rows * scale * ffn_gain).astype(jnp.bfloat16)
    residual_own = lax.dynamic_slice_in_dim(full_rows, offset, local_cols, 1)
    pieces = in_one_piece((w_gate, w_value), SP, 0, 1)
    gate = jnp.dot(normed_rows, pieces[0], preferred_element_type=jnp.float32)
    value = jnp.dot(normed_rows, pieces[1], preferred_element_type=jnp.float32)
    gate = gate.astype(jnp.bfloat16)
    value = value.astype(jnp.bfloat16)
    edge = passed_along(gate[tokens - 2 :], SP, 1)
    extended = jnp.concatenate([edge, gate], axis=0).astype(jnp.float32)
    ids = jnp.concatenate([incoming[5], incoming[4], seg])
    near = (ids[1:-1] == seg)[:, None]
    far = (ids[:-2] == seg)[:, None]
    conv = (
        conv_taps[2] * extended[2:]
        + conv_taps[1] * jnp.where(near, extended[1:-1], 0.0)
        + conv_taps[0] * jnp.where(far, extended[:-2], 0.0)
    )
    hidden = (jax.nn.silu(conv) * value.astype(jnp.float32)).astype(jnp.bfloat16)
    terms = jnp.dot(
        hidden, lax.all_gather(w_down, SP, axis=1, tiled=True), preferred_element_type=jnp.float32
    )
    down = lax.psum_scatter(
        terms.astype(jnp.bfloat16), "tp", scatter_dimension=1, tiled=True
    ).astype(jnp.float32)
    return (residual_own + down).astype(jnp.bfloat16)


def solution(mesh):
    torus = Mesh(mesh.devices.reshape(4, 4, mesh.shape["tp"]), ("sp_0", "sp_1", "tp"))
    placed = (
        P(SP, "tp"),
        P(SP, "tp"),
        P(SP, "tp"),
        P(SP, "tp"),
        P(SP, "tp"),
        P("tp", SP),
        P("tp", SP),
        P(SP),
        P("tp"),
        P("tp", None),
        P(),
        P(SP, "tp"),
        P(SP, "tp"),
        P(None, "tp"),
        P("tp", SP),
    )
    return jax.shard_map(body, mesh=torus, in_specs=placed, out_specs=P(SP, "tp"), check_vma=False)
```

profile of v0, /device:TPU:0, one launch (start us, length us, event | category | flops | bytes accessed | tf_op | source)
XLA Modules:
  0.0 438.6 jit_solution(1473426285927869053)
XLA Ops:
  8.6 6.3 %fusion.104 = f32[12,64,2]{2,0,1:T(8,128)S(1)} fusion(f32[12,64,2]{2,0,1:T(8,128)S(1)} %copy.338), kind=kOutput, calls=%fused_computation.244 | output fusion | flops 96768 | bytes 12288 | tf_op jit(solution)/shard_map/jit(cumsum)/reduce_window_sum | solution.py:111
  19.5 1.4 reshape.907
  20.9 1.3 copy.349
  22.3 1.6 broadcast_multiply_fusion.1
  23.9 1.3 fusion.37
  25.3 94.5 %while.32 = (s32[]{:T(128)}, f32[2,96,96]{2,1,0:T(8,128)S(1)}, f32[2]{0:T(128)S(1)}, f32[2]{0:T(128)S(1)}, f32[1]{0:T(128)}, /*index=5*/f32[1]{0:T(128)}, f32[1]...) while((s32[]{:T(128)}, f32[2,96,96]{2,1,0:T(8,128)S(1)}, ...), condition=%wide.region_4.5_spmd.clone.clone, body=%wide.region_3.4_spmd.clone.sunk.clone | while | flops 92189 | bytes 394247 | solution.py:179
  90.8 1.3 dynamic_update_slice.40
  92.1 1.3 dynamic_update_slice.41
  98.7 1.3 dynamic_update_slice.40
  100.0 1.3 dynamic_update_slice.41
  107.9 1.3 dynamic_update_slice.41
  115.7 1.3 dynamic_update_slice.41
  120.7 13.0 %all-gather.2 = f32[4,197,96]{1,2,0:T(8,128)S(1)} all-gather(f32[1,197,96]{1,2,0:T(8,128)S(1)} %bitcast.367), channel_id=2, replica_groups=mesh['sp_0'=4,'sp_1'=4,'tp'=8] {'sp_1'}, dimensions={0}, use_global_device_ids=true | all-gather | bytes 378240 | tf_op jit(solution)/shard_map/all_gather | solution.py:31
  151.3 14.3 %all-gather.3 = f32[4,197,96]{1,2,0:T(8,128)S(1)} all-gather(f32[1,197,96]{1,2,0:T(8,128)S(1)} %bitcast.368), channel_id=3, replica_groups=mesh['sp_0'=4,'sp_1'=4,'tp'=8] {'sp_0'}, dimensions={0}, use_global_device_ids=true | all-gather | bytes 378240 | tf_op jit(solution)/shard_map/all_gather | solution.py:31
  185.4 1.7 fusion.33
  187.1 2.6 multiply_reduce_fusion.1
  193.0 1.4 convolution_convert_fusion.1
  194.5 4.9 %convert_element_type.66 = f32[768,3072]{1,0:T(8,128)} convert(bf16[768,3072]{1,0:T(8,128)(2,1)S(1)} %convolution_convert_fusion.1) | non-fusion elementwise | flops 2359296 | bytes 14155776 | tf_op jit(solution)/shard_map/convert_element_type | solution.py:193
  199.4 2.5 add_dynamic-update-slice_fusion
  208.3 108.6 %all-reduce.12.cloned.1.call-done = f32[768,3072]{1,0:T(8,128)} async-done(((f32[768,3072]{1,0:T(8,128)}), f32[768,3072]{1,0:T(8,128)}) %all-reduce.12.cloned.1.call-update) | async-done | bytes 9437200 | tf_op jit(solution)/shard_map/psum | solution.py:199
  316.9 4.5 %multiply_reduce_fusion = f32[768]{0:T(1024)S(1)} fusion(f32[768,3072]{1,0:T(8,128)} %all-reduce.12.cloned.1.call-done), kind=kLoop, calls=%fused_computation.21 | loop fusion | flops 4717824 | bytes 9440256 | tf_op jit(solution)/shard_map/reduce_sum | solution.py:200
  321.5 11.5 %fusion.12 = bf16[768,1056]{0,1:T(8,128)(2,1)S(1)} fusion(bf16[3072,2112]{1,0:T(8,128)(2,1)} %all-gather.7.cloned.1.call-done, f32[768,3072]{1,0:T(8,128)} %all-reduce.12.cloned.1.call-done, f32[3072]{0:T(1024)S(1)} %copy-done.33, f32[768]{0:T(1024)S(1)} %add_rsqrt_fusion.1), kind=kOutput, calls=%fused_computation.28 | convolution fusion | flops 4990722048 | bytes 18152448 | tf_op jit(solution)/shard_map/dot_general | solution.py:204
  333.1 3.6 collective-permute-start
  336.8 11.9 %collective-permute-done = bf16[2,1056]{0,1:T(8,128)(2,1)S(1)} collective-permute-done((bf16[2,1056]{0,1:T(8,128)(2,1)S(1)}, bf16[2,1056]{0,1:T(8,128)(2,1)S(1)}, u32[]{:S(2)}, u32[]{:S(2)}) %collective-permute-start) | collective-permute-done | bytes 4256 | tf_op jit(solution)/shard_map/ppermute | solution.py:65
  348.6 2.6 maximum_convert_fusion
  351.3 18.2 %fusion.24 = bf16[768,1056]{0,1:T(8,128)(2,1)S(1)} fusion(bf16[3072,2112]{1,0:T(8,128)(2,1)} %all-gather.7.cloned.1.call-done, f32[770,1056]{0,1:T(8,128)} %maximum_convert_fusion, f32[1056]{0:T(1024)S(1)} %get-tuple-element.330, f32[1056]{0:T(1024)S(1)} %get-tuple-element.331, f32[1056]{0:T(1024)S(1)} %get-tuple-element.329, ...), kind=kOutput, calls=%fused_computation.32 | convolution fusion | flops 5002076160 | bytes 27898752 | tf_op jit(solution)/shard_map/dot_general | solution.py:205
  369.5 1.5 all-gather.9.cloned.1.call-done
  371.0 11.1 %convolution_convert_fusion = bf16[768,3072]{1,0:T(8,128)(2,1)} fusion(bf16[768,1056]{0,1:T(8,128)(2,1)S(1)} %fusion.24, bf16[1056,3072]{0,1:T(8,128)(2,1)} %all-gather.9.cloned.1.call-done), kind=kOutput, calls=%fused_computation.26 | convolution fusion | flops 4985192448 | bytes 12828672 | tf_op jit(solution)/shard_map/dot_general | solution.py:219
  382.1 6.6 %copy.389 = bf16[768,3072]{0,1:T(8,128)(2,1)} copy(bf16[768,3072]{1,0:T(8,128)(2,1)} %convolution_convert_fusion) | data formatting | bytes 9437184
  388.8 38.8 %reduce-scatter.4.cloned.1.call-done = bf16[384,768]{1,0:T(8,128)(2,1)} async-done(((bf16[3072,768]{1,0:T(8,128)(2,1)}), bf16[384,768]{1,0:T(8,128)(2,1)}) %reduce-scatter.4.cloned.1.call-update) | async-done | bytes 589840
  427.6 1.4 copy.390
  429.0 2.2 add_convert_fusion
  (327 shorter events, 80.2 us)
Async XLA Ops:
  7.4 185.6 %copy-start = (bf16[192,3072]{1,0:T(8,128)(2,1)S(1)}, bf16[192,3072]{1,0:T(8,128)(2,1)}, u32[]{:S(2)}) copy-start(bf16[192,3072]{1,0:T(8,128)(2,1)} %param.26) | copy-start | bytes 3538948
  7.4 309.5 %all-reduce.12.cloned.1.call-start = ((), (), s32[]{:S(2)}) async-start(), calls=%async_computation.1 | async-start | bytes 18874368 | tf_op jit(solution)/shard_map/psum | solution.py:199
  17.5 158.7 %copy-start.11 = (f32[12,64,2]{1,2,0:T(2,128)}, f32[12,64,2]{1,2,0:T(2,128)S(1)}, u32[]{:S(2)}) copy-start(f32[12,64,2]{1,2,0:T(2,128)S(1)} %get-tuple-element.393) | copy-start | bytes 18436
  120.6 54.9 %copy-start.15 = (f32[12,2]{1,0:T(8,128)S(1)}, f32[12,2]{1,0:T(8,128)}, u32[]{:S(2)}) copy-start(f32[12,2]{1,0:T(8,128)} %get-tuple-element.116) | copy-start | bytes 292
  120.6 55.0 %copy-start.16 = (f32[12,2]{1,0:T(8,128)S(1)}, f32[12,2]{1,0:T(8,128)}, u32[]{:S(2)}) copy-start(f32[12,2]{1,0:T(8,128)} %get-tuple-element.115) | copy-start | bytes 292
  120.6 55.1 %copy-start.30 = (f32[12,1]{0,1:T(1,128)S(1)}, f32[12,1]{0,1:T(1,128)}, u32[]{:S(2)}) copy-start(f32[12,1]{0,1:T(1,128)} %copy-done.29) | copy-start | bytes 148
  120.6 55.3 %copy-start.32 = (f32[12,1]{0,1:T(1,128)S(1)}, f32[12,1]{0,1:T(1,128)}, u32[]{:S(2)}) copy-start(f32[12,1]{0,1:T(1,128)} %copy-done.31) | copy-start | bytes 148
  147.0 34.6 %copy-start.10 = (bf16[768,192]{0,1:T(8,128)(2,1)S(1)}, bf16[768,192]{0,1:T(8,128)(2,1)}, u32[]{:S(2)}) copy-start(bf16[768,192]{0,1:T(8,128)(2,1)} %param.18) | copy-start | bytes 884740
  149.2 1.9 copy-start.26
  149.3 1.2 copy-start.21
  149.3 1.3 copy-start.19
  149.3 1.4 copy-start.22
  166.7 17.4 %copy-start.18 = (f32[2]{0:T(128)S(1)}, f32[2]{0:T(128)}, u32[]{:S(2)}) copy-start(f32[2]{0:T(128)} %copy-done.17) | copy-start | bytes 28
  175.9 6.7 %copy-start.27 = (f32[2]{0:T(128)S(1)}, f32[2]{0:T(128)}, u32[]{:S(2)}) copy-start(f32[2]{0:T(128)} %get-tuple-element.377) | copy-start | bytes 28
  176.2 5.3 %copy-start.9 = (pred[12,64,64]{1,2,0:T(8,128)(4,1)}, pred[12,64,64]{1,2,0:T(8,128)(4,1)S(1)}, u32[]{:S(2)}) copy-start(pred[12,64,64]{1,2,0:T(8,128)(4,1)S(1)} %compare_and_fusion) | copy-start | bytes 147460
  176.2 6.4 %copy-start.28 = (f32[2]{0:T(128)S(1)}, f32[2]{0:T(128)}, u32[]{:S(2)}) copy-start(f32[2]{0:T(128)} %get-tuple-element.381) | copy-start | bytes 28
  176.2 7.9 %copy-start.25 = (f32[2]{0:T(128)S(1)}, f32[2]{0:T(128)}, u32[]{:S(2)}) copy-start(f32[2]{0:T(128)} %get-tuple-element.376) | copy-start | bytes 28
  178.2 5.9 %copy-start.6 = (f32[1,192,96]{2,1,0:T(8,128)S(1)}, f32[1,192,96]{2,1,0:T(8,128)}, u32[]{:S(2)}) copy-start(f32[1,192,96]{2,1,0:T(8,128)} %copy.372) | copy-start | bytes 221188
  179.0 5.1 %copy-start.7 = (f32[1,192,96]{2,1,0:T(8,128)S(1)}, f32[1,192,96]{2,1,0:T(8,128)}, u32[]{:S(2)}) copy-start(f32[1,192,96]{2,1,0:T(8,128)} %copy.373) | copy-start | bytes 221188
  179.7 4.4 %copy-start.8 = (f32[1,192,96]{2,1,0:T(8,128)S(1)}, f32[1,192,96]{2,1,0:T(8,128)}, u32[]{:S(2)}) copy-start(f32[1,192,96]{2,1,0:T(8,128)} %copy.374) | copy-start | bytes 221188
  180.5 6.6 %copy-start.2 = (bf16[12,64,2,96]{3,1,2,0:T(8,128)(2,1)S(1)}, bf16[12,64,2,96]{3,1,2,0:T(8,128)(2,1)}, u32[]{:S(2)}) copy-start(bf16[12,64,2,96]{3,1,2,0:T(8,128)(2,1)} %copy.349) | copy-start | bytes 884740
  189.7 3.4 copy-start.34
  194.5 5.0 %copy-start.3 = (bf16[768,384]{1,0:T(8,128)(2,1)S(1)}, bf16[768,384]{1,0:T(8,128)(2,1)}, u32[]{:S(2)}) copy-start(bf16[768,384]{1,0:T(8,128)(2,1)} %param.17) | copy-start | bytes 1769476
  201.9 3.2 copy-start.14
  201.9 6.4 %copy-start.12 = (s32[768]{0:T(1024)S(1)}, s32[768]{0:T(1024)}, u32[]{:S(2)}) copy-start(s32[768]{0:T(1024)} %param.24) | copy-start | bytes 9220
  202.0 119.5 %all-gather.7.cloned.1.call-start = ((), (), s32[]{:S(2)}) async-start(), calls=%async_computation.2 | async-start | bytes 14204928 | tf_op jit(solution)/shard_map/all_gather | solution.py:58
  204.2 166.8 %all-gather.9.cloned.1.call-start = ((), (), s32[]{:S(2)}) async-start(), calls=%async_computation.3 | async-start | bytes 7520256 | tf_op jit(solution)/shard_map/all_gather | solution.py:220
  204.8 222.8 %reduce-scatter.4.cloned.1.call-start = ((), (), s32[]{:S(2)}) async-start(), calls=%async_computation.4 | async-start | bytes 5308416
  208.3 113.1 %copy-start.33 = (f32[3072]{0:T(1024)S(1)}, f32[3072]{0:T(1024)}, u32[]{:S(2)}) copy-start(f32[3072]{0:T(1024)} %param.27) | copy-start | bytes 36868
  321.4 15.3 %copy-start.13 = (f32[3,1056]{1,0:T(4,128)S(1)}, f32[3,1056]{1,0:T(4,128)}, u32[]{:S(2)}) copy-start(f32[3,1056]{1,0:T(4,128)} %param.30) | copy-start | bytes 38020
  333.1 15.5 %collective-permute-start = (bf16[2,1056]{0,1:T(8,128)(2,1)S(1)}, bf16[2,1056]{0,1:T(8,128)(2,1)S(1)}, u32[]{:S(2)}, u32[]{:S(2)}) collective-permute-start(bf16[2,1056]{0,1:T(8,128)(2,1)S(1)} %slice.379), channel_id=1, source_target_pairs={{0,8},{8,16},{16,24},{24,32},{32,40},{40,48},{48,56},{56,64},{64,7... | collective-permute-start | bytes 12680 | tf_op jit(solution)/shard_map/ppermute | solution.py:65
  388.8 42.4 %copy-start.1 = (bf16[192,3072]{1,0:T(8,128)(2,1)S(1)}, bf16[192,3072]{1,0:T(8,128)(2,1)}, u32[]{:S(2)}) copy-start(bf16[192,3072]{1,0:T(8,128)(2,1)} %param.26) | copy-start | bytes 3538948
  (8 other events, 6.5 us)
Sparse Core Ops, SparseCore 0:
  202.1 114.7 all-reduce.11
  388.9 38.6 reduce-scatter.3
Sparse Core Ops, SparseCore 1:
  204.6 94.4 all-gather.6
  301.0 70.0 all-gather.8
where the time goes:
time: 441 us; the launch traced here: 439 us
  waiting for transfers between devices  161 us (37%)
  local copies, waits for them, and re-layouts  80 us (18%)
  matrix products  47.9 us (11%)
  other arithmetic  42.4 us (10%)
  loops' own time  38.2 us (9%)
  between operations  37.6 us (9%)
  blocking collectives  27.3 us (6%)
    psum x1, waiting for transfers between devices, body(): full_rows = lax.psum(term + placed, 'tp')  109 us
    unnamed x5, waiting for transfers between devices  39.4 us
    another operation x1, loops' own time, body(): local_end, before = lax.scan(advance, empty_state(heads, DH), elements)  38.2 us
    dynamic_update_slice x48, local copies, waits for them, and re-layouts, body(): local_end, before = lax.scan(advance, empty_state(heads, DH), elements)  33.1 us
    all_gather x2, blocking collectives, collected_together(): both, at, found = (lax.all_gather(jnp.concatenate(lines), axis), 0, {})  27.3 us
    dot_general x1, matrix products, body(): value = jnp.dot(normed_rows, pieces[1], preferred_element_type=jnp.float32)  18.2 us
    dynamic_slice x24, local copies, waits for them, and re-layouts, body(): local_end, before = lax.scan(advance, empty_state(heads, DH), elements)  13.8 us
    ppermute x1, waiting for transfers between devices, passed_along(): lax.ppermute(value, axis, [(source, source + steps) for source in range(i...  11.9 us
  transfers between devices with their start and end apart: 5, of which 4 were waited for; matrix products, arithmetic and copies ran while one was open for 9% of the time, Pallas kernels for 0%

commit v1 on v0

v1 whole, which is shorter than its diff:
```python
import jax
import jax.numpy as jnp
from jax import lax
from jax.experimental import pallas as pl
from jax.experimental.pallas import tpu as pltpu
from jax.sharding import Mesh
from jax.sharding import PartitionSpec as P

MESH = pl.DeviceIdType.MESH
F32 = jnp.float32
BF16 = jnp.bfloat16
ABSENT = -1e30
DH = 96
TOK = 768
OWN = 384
HW = 192
MAIN = 1024
GW = 1152
LANES = 3200
DOWN0 = 2176
EPS = 1e-6
SEMS = 160

GATE_P = dict(rows=(0, 192), lanes=(0, GW), cut=(96, 96), first="x")
VALUE_P = dict(rows=(0, 192), lanes=(GW, MAIN), cut=(96, 96), first="z")
DOWN_A = dict(rows=(0, 96), lanes=(DOWN0, MAIN), cut=(48, 48), first="x")
DOWN_B = dict(rows=(96, 96), lanes=(DOWN0, MAIN), cut=(48, 48), first="z")


def mod4(v):
    return lax.rem(v + 8, 4)


def dot(a, b, **kw):
    return lax.dot_general(a, b, (((1,), (0,)), ((), ())), preferred_element_type=F32, **kw)


def dot_t(a, b, **kw):
    return lax.dot_general(a, b, (((1,), (1,)), ((), ())), preferred_element_type=F32, **kw)


def kernel(
    pk,
    q_ref,
    k_ref,
    v_ref,
    og_ref,
    gates_ref,
    wo_ref,
    resid_ref,
    hg_ref,
    gain_ref,
    taps_ref,
    out_ref,
    W,
    X,
    MIX,
    WO,
    VP,
    OI,
    MF,
    NF,
    ST,
    SR,
    SS,
    RES,
    GT,
    EDGE,
    HD,
    SP,
    RP,
    PO,
    ZS,
    RL,
    RV,
    ssem,
    rsem,
    lsem,
):
    z, x = lax.axis_index("z"), lax.axis_index("x")
    y, c = lax.axis_index("y"), lax.axis_index("c")
    sp = z * 4 + x
    tp = y * 2 + c
    o = 1 - c
    table = {}
    started = []

    def slot(key):
        return table.setdefault(key, len(table))

    def send(key, src, dst, dev):
        i = slot(key)
        d = pltpu.make_async_remote_copy(
            src_ref=src,
            dst_ref=dst,
            send_sem=ssem.at[i],
            recv_sem=rsem.at[i],
            device_id=dev,
            device_id_type=MESH,
        )
        d.start()
        started.append(d)

    def recv(key, dst):
        i = slot(key)
        pltpu.make_async_remote_copy(
            src_ref=dst,
            dst_ref=dst,
            send_sem=ssem.at[i],
            recv_sem=rsem.at[i],
            device_id=(z, x, y, o),
            device_id_type=MESH,
        ).wait_recv()

    def at_sp(n):
        s = lax.rem(sp + n + 16, 16)
        return (s // 4, lax.rem(s, 4), y, c)

    def at_x(d):
        return (z, mod4(x + d), y, c)

    def at_z(d):
        return (mod4(z + d), x, y, c)

    def at_y(d):
        return (z, x, mod4(y + d), c)

    def at_tp(n):
        t = lax.rem(tp + n, 8)
        return (z, x, t // 2, lax.rem(t, 2))

    partner = (z, x, y, o)

    peers = [at_x(1), at_x(-1), at_z(1), at_z(-1)]
    peers += [at_tp(n) for n in range(1, 8)]
    peers += [at_sp(n) for n in (1, 2, 3, -1, -2, -3)]
    barrier = pltpu.get_barrier_semaphore()
    for dev in peers:
        pl.semaphore_signal(barrier, inc=1, device_id=dev, device_id_type=MESH)
    pl.semaphore_wait(barrier, len(peers))

    def place(part, dp, ds, half=None):
        if part["first"] == "x":
            zz, xx = mod4(z + ds), mod4(x + dp)
        else:
            zz, xx = mod4(z + dp), mod4(x + ds)
        r0, nr = part["rows"]
        if half is not None:
            r0, nr = r0 + (part["cut"][0] if half else 0), part["cut"][half]
        row = pl.multiple_of((zz * 4 + xx) * HW + r0, 16)
        l0, nl = part["lanes"]
        return W.at[pl.ds(row, nr), pl.ds(l0, nl)]

    def stage(name, part):
        first = part["first"] == "x"
        prim = at_x if first else at_z
        secd = at_z if first else at_x
        steps = (0, -1, 1, 2)

        def own():
            r0, nr = part["rows"]
            l0, nl = part["lanes"]
            src = pk.at[pl.ds(r0, nr), pl.ds(l0, nl)]
            dst = place(part, 0, 0)
            for d in (1, -1):
                send((name, "p", d), src, dst, prim(d))
            for d in (1, -1):
                send((name, "s", d, 0), src, dst, secd(d))

        def second(m):
            dst = place(part, steps[m], 0)
            for d in (1, -1):
                send((name, "s", d, m), dst, dst, secd(d))

        def e1():
            for d in (1, -1):
                recv((name, "p", d), place(part, -d, 0))
                half = 0 if d == 1 else 1
                piece = place(part, -d, 0, half)
                send((name, "pf", d), piece, piece, prim(d))
            second(1)
            second(2)

        def across(m):
            for d in (1, -1):
                recv((name, "s", d, m), place(part, steps[m], -d))
                half = 0 if d == 1 else 1
                piece = place(part, steps[m], -d, half)
                send((name, "sf", d, m), piece, piece, secd(d))

        def e3():
            for d in (1, -1):
                recv((name, "pf", d), place(part, 2, 0, 0 if d == 1 else 1))
            second(3)

        def e7():
            for m in range(4):
                for d in (1, -1):
                    recv((name, "sf", d, m), place(part, steps[m], 2, 0 if d == 1 else 1))

        return [own, e1, lambda: across(0), e3, lambda: across(1), lambda: across(2), lambda: across(3), e7]

    def pair(a, b):
        return [lambda f=f, g=g: (f(), g()) for f, g in zip(a, b)]

    gv = pair(stage("g", GATE_P), stage("v", VALUE_P))
    dn = pair(stage("da", DOWN_A), stage("db", DOWN_B))

    def over_tp(name, blk):
        def g0():
            b = blk(y, c)
            send((name, "o"), b, b, partner)
            for d in (1, -1):
                send((name, "y", d), b, b, at_y(d))

        def g1():
            for d in (1, -1):
                src = mod4(y - d)
                recv((name, "y", d), blk(src, c))
                h = blk(src, c, 0 if d == 1 else 1)
                send((name, "f", d), h, h, at_y(d))
                send((name, "of", d), blk(src, c), blk(src, c), partner)

        def g2():
            far = mod4(y + 2)
            for d in (1, -1):
                h = blk(far, c, 0 if d == 1 else 1)
                recv((name, "f", d), h)
                send((name, "oh", d), h, h, partner)

        def g3():
            far = mod4(y + 2)
            recv((name, "o"), blk(y, o))
            for d in (1, -1):
                recv((name, "of", d), blk(mod4(y - d), o))
                recv((name, "oh", d), blk(far, o, 0 if d == 1 else 1))

        return g0, g1, g2, g3

    def block_of(ref, width):
        def blk(yy, cc, half=None):
            rows = slice(None) if half is None else pl.ds(half * OWN, OWN)
            return ref.at[rows, pl.ds(pl.multiple_of((yy * 2 + cc) * width, 128), width)]

        return blk

    mix_g = over_tp("m", block_of(MIX, 256))
    x_g = over_tp("x", block_of(X, OWN))

    gv[0]()
    for n in range(1, 8):
        t = lax.rem(tp + n, 8)
        src = wo_ref.at[:, pl.ds(pl.multiple_of(t * OWN, 128), OWN)]
        dst = WO.at[pl.ds(pl.multiple_of(tp * 256, 16), HW), :]
        send(("w", n), src, dst, at_tp(n))
    local_w = pltpu.make_async_copy(
        pk, W.at[pl.ds(pl.multiple_of(sp * HW, 16), HW), :], lsem.at[0]
    )
    local_w.start()
    local_o = pltpu.make_async_copy(
        wo_ref.at[:, pl.ds(pl.multiple_of(tp * OWN, 128), OWN)],
        WO.at[pl.ds(pl.multiple_of(tp * 256, 16), HW), :],
        lsem.at[1],
    )
    local_o.start()
    for j in range(8):
        WO[j * 256 + HW : (j + 1) * 256, :] = jnp.zeros((64, OWN), BF16)

    gates = gates_ref[...]
    lane = lax.broadcasted_iota(jnp.int32, (8, TOK), 1)
    row8 = lax.broadcasted_iota(jnp.int32, (8, TOK), 0)
    e = jnp.exp(-jnp.abs(gates))
    log1p = jnp.where(e < 1e-2, e * (1.0 - e * (0.5 - e * (1.0 / 3.0))), jnp.log(1.0 + e))
    cum = jnp.minimum(gates, 0.0) - log1p
    shift = 1
    while shift < TOK:
        cum = cum + jnp.where(lane >= shift, pltpu.roll(cum, shift, 1), 0.0)
        shift *= 2
    seg = gates[4:5]
    b = [gates[h : h + 1] - cum[2 + h : 3 + h] for h in range(2)]
    end = [cum[2 + h : 3 + h, TOK - 1 :] for h in range(2)]
    first, last, second_last = seg[:, :1], seg[:, TOK - 1 :], seg[:, TOK - 2 : TOK - 1]
    rows = jnp.where(row8 == 0, b[0], jnp.where(row8 == 1, b[1], seg))
    cols = jnp.transpose(jnp.concatenate([rows, jnp.zeros((120, TOK), F32)], axis=0))
    seg_c = cols[:, 2:3]
    lane256 = lax.broadcasted_iota(jnp.int32, (TOK, 256), 1)
    in0 = lane256 < DH
    in1 = (lane256 >= DH) & (lane256 < HW)

    VP[...] = jnp.zeros_like(VP)
    VP[:, 0:HW] = v_ref[...]
    keys = k_ref[...]
    lane_k = lax.broadcasted_iota(jnp.int32, (TOK, HW), 1)
    zero_k = jnp.zeros_like(keys)
    key_h = [jnp.where(lane_k < DH, keys, zero_k), jnp.where(lane_k < DH, zero_k, keys)]
    peak = []
    weight = []
    for h in range(2):
        top = jnp.max(jnp.where(seg == last, b[h], ABSENT), axis=1, keepdims=True)
        peak.append(top)
        weight.append(jnp.where(seg_c == last, jnp.exp(jnp.minimum(cols[:, h : h + 1] - top, 0.0)), 0.0))
    scaled = keys.astype(F32) * (jnp.where(lane_k < DH, weight[0], weight[1]) * DH**-0.5)
    state = lax.dot_general(
        scaled.astype(BF16), VP[...], (((0,), (0,)), ((), ())), preferred_element_type=F32
    )
    r192 = lax.broadcasted_iota(jnp.int32, (HW, 128), 0)
    l192 = lax.broadcasted_iota(jnp.int32, (HW, 128), 1)
    folded = jnp.where(r192 < DH, state[:, :128], pltpu.roll(state, 256 - DH, 1)[:, :128])
    ST[0:HW, :] = jnp.where(l192 < DH, folded, 0.0)
    meta_row = lax.broadcasted_iota(jnp.int32, (8, 128), 0)
    meta = jnp.zeros((8, 128), F32)
    for n, value in enumerate((end[0] + peak[0], end[1] + peak[1], end[0], end[1], first, last, second_last)):
        meta = jnp.where(meta_row == n, value, meta)
    ST[HW : HW + 8, :] = meta
    for n in range(1, 5):
        send(("st", n), ST, SR.at[n - 1], at_sp(n))

    for i in range(3):
        t0, ns = i * 256, (i + 1) * 256
        qb = q_ref[t0 : t0 + 256, :]
        s_at = lax.broadcasted_iota(jnp.int32, (256, ns), 1)
        t_at = lax.broadcasted_iota(jnp.int32, (256, ns), 0) + t0
        mask = (seg_c[t0 : t0 + 256] == seg[:, :ns]) & (s_at <= t_at)
        parts, tops = [], []
        for h in range(2):
            masked = jnp.where(mask, b[h][:, :ns], ABSENT)
            top = jnp.max(masked, axis=1, keepdims=True)
            scores = dot_t(qb, key_h[h][:ns]) * (jnp.exp(masked - top) * DH**-0.5)
            parts.append(dot(scores.astype(BF16), VP[0:ns, :]))
            tops.append(top)
        left = in0[t0 : t0 + 256]
        OI[t0 : t0 + 256, :] = jnp.where(left, parts[0], parts[1])
        MF[t0 : t0 + 256, :] = jnp.where(left, tops[0], tops[1])

    gv[1]()

    dec = [jnp.zeros((1, 128), F32)] * 2
    cand = [[], []]
    first_l = jnp.broadcast_to(first, (1, 128))
    for n in range(1, 5):
        recv(("st", n), SR.at[n - 1])
        m = SR[n - 1, HW : HW + 8, :]
        valid = (m[5:6] == first_l) & (sp >= n)
        for h in range(2):
            cand[h].append(jnp.where(valid, m[h : h + 1] + dec[h], ABSENT))
            dec[h] = dec[h] + m[2 + h : 3 + h]
    pin = [jnp.maximum(jnp.maximum(p[0], p[1]), jnp.maximum(p[2], p[3])) for p in cand]
    carried = jnp.zeros((HW, 128), F32)
    for n in range(4):
        f = [jnp.exp(cand[h][n] - pin[h]) for h in range(2)]
        carried = carried + jnp.where(r192 < DH, f[0], f[1]) * SR[n, 0:HW, :]
    wide = jnp.concatenate([carried, jnp.zeros((HW, 128), F32)], axis=1)
    r256 = lax.broadcasted_iota(jnp.int32, (HW, 256), 0)
    spread = jnp.where(r256 < DH, wide, pltpu.roll(wide, DH, 1)).astype(BF16)
    inter = dot(q_ref[...], spread)
    pin_l = jnp.where(in0, pin[0][:, :1], pin[1][:, :1])
    pin_t = jnp.where(seg_c == first, pin_l, ABSENT)
    top = jnp.maximum(MF[...], pin_t)
    memory = jnp.exp(MF[...] - top) * OI[...] + jnp.exp(pin_t - top) * inter
    square = memory * memory
    mean0 = jnp.sum(jnp.where(in0, square, 0.0), axis=1, keepdims=True) * (1.0 / DH)
    mean1 = jnp.sum(jnp.where(in1, square, 0.0), axis=1, keepdims=True) * (1.0 / DH)
    normed = memory * lax.rsqrt(jnp.where(in0, mean0, mean1) + 1.0)
    mix = normed[:, :HW] * hg_ref[...] * jax.nn.sigmoid(og_ref[...].astype(F32))
    own_mix = pl.multiple_of(tp * 256, 128)
    MIX[:, pl.ds(own_mix, 256)] = jnp.zeros((TOK, 256), BF16)
    VP[:, 0:HW] = mix.astype(BF16)
    MIX[:, pl.ds(own_mix, 256)] = VP[...]
    mix_g[0]()

    before = SR[0, HW : HW + 8, :]
    there = sp >= 1
    last_before = jnp.where(there, before[5:6, :1], -1.0)
    second_before = jnp.where(there, before[6:7, :1], -1.0)
    one_back = jnp.where(lane == 0, last_before, pltpu.roll(gates, 1, 1))[4:5]
    two_back = jnp.where(
        lane == 0, second_before, jnp.where(lane == 1, last_before, pltpu.roll(gates, 2, 1))
    )[4:5]
    flags = jnp.where(
        row8 == 0, jnp.where(one_back == seg, 1.0, 0.0), jnp.where(two_back == seg, 1.0, 0.0)
    )
    NF[...] = jnp.transpose(jnp.concatenate([flags, jnp.zeros((120, TOK), F32)], axis=0))

    gv[2]()
    gv[3]()
    mix_g[1]()
    mix_g[2]()
    gv[4]()
    mix_g[3]()

    local_o.wait()
    for n in range(1, 8):
        t = lax.rem(tp + 8 - n, 8)
        recv(("w", n), WO.at[pl.ds(pl.multiple_of(t * 256, 16), HW), :])
    gain = gain_ref[:, pl.ds(pl.multiple_of(tp * OWN, 128), OWN)]
    res = resid_ref[...].astype(F32) + dot(MIX[...], WO[...])
    RES[...] = res
    X[:, pl.ds(pl.multiple_of(tp * OWN, 128), OWN)] = (res * gain).astype(BF16)
    SS[tp] = dot_t(jnp.ones((8, OWN), F32), res * res, precision=lax.Precision.HIGHEST)
    x_g[0]()
    for n in range(1, 8):
        send(("q", n), SS.at[tp], SS.at[tp], at_tp(n))
    gv[5]()
    x_g[1]()
    gv[6]()
    dn[0]()
    x_g[2]()
    x_g[3]()
    total = SS[tp]
    for n in range(1, 8):
        t = lax.rem(tp + 8 - n, 8)
        recv(("q", n), SS.at[t])
        total = total + SS[t]
    scale_row = lax.rsqrt(total * (1.0 / 3072.0) + EPS)
    OI[:, 0:128] = jnp.transpose(jnp.concatenate([scale_row, jnp.zeros((120, TOK), F32)], axis=0))
    local_w.wait()
    gv[7]()
    dn[1]()

    scale = OI[:, 0:1]

    def gate_tile(n, _):
        l = pl.ds(pl.multiple_of(n * 256, 256), 256)
        GT[:, l] = (dot(X[...], W[:, l]) * scale).astype(BF16)
        return 0

    lax.fori_loop(0, 4, gate_tile, 0)
    GT[:, MAIN:GW] = (dot(X[...], W[:, MAIN:GW]) * scale).astype(BF16)
    send(("e",), GT.at[TOK - 16 : TOK, :], EDGE, at_sp(1))
    dn[2]()
    dn[3]()

    def hidden_of(lanes, width, value):
        g = GT[:, lanes].astype(F32)
        edge = EDGE[:, lanes].astype(F32)
        taps = taps_ref[:, lanes]
        t_at = lax.broadcasted_iota(jnp.int32, (TOK, width), 0)
        near = NF[:, 0:1] > 0.5
        far = NF[:, 1:2] > 0.5
        g1 = jnp.where(t_at == 0, edge[15:16], pltpu.roll(g, 1, 0))
        g2 = jnp.where(
            t_at == 0, edge[14:15], jnp.where(t_at == 1, edge[15:16], pltpu.roll(g, 2, 0))
        )
        conv = taps[2:3] * g + taps[1:2] * jnp.where(near, g1, 0.0) + taps[0:1] * jnp.where(far, g2, 0.0)
        return conv / (1.0 + jnp.exp(-conv)) * value

    recv(("e",), EDGE)

    def value_tile(n, _):
        l = pl.ds(pl.multiple_of(n * 256, 256), 256)
        w = pl.ds(pl.multiple_of(n * 256 + GW, 128), 256)
        value = (dot(X[...], W[:, w]) * scale).astype(BF16).astype(F32)
        HD[:, l] = hidden_of(l, 256, value).astype(BF16)
        return 0

    lax.fori_loop(0, 4, value_tile, 0)
    tail = slice(MAIN, GW)
    value_tail = pltpu.roll(GT[:, tail].astype(F32), 96, 1)
    HD[:, tail] = pltpu.roll(hidden_of(tail, 128, value_tail), 64, 1).astype(BF16)
    dn[4]()
    dn[5]()
    dn[6]()
    dn[7]()

    def partial(yy, cc):
        r = pl.ds(pl.multiple_of((yy * 2 + cc) * OWN, 128), OWN)
        return dot_t(HD[:, 0:MAIN], W[r, DOWN0:LANES]) + dot_t(HD[:, MAIN:GW], W[r, MAIN:GW])

    order = (2, 1, -1, 0)
    for n, d in enumerate(order):
        yy = mod4(y + d)
        SP[n] = partial(yy, o).astype(BF16)
        send(("sp", n), SP.at[n], RP.at[n], partner)
        PO[n % 2] = partial(yy, c)
        recv(("sp", n), RP.at[n])
        both = PO[n % 2] + RP[n].astype(F32)
        if d == 2:
            ZS[0] = both.astype(BF16)
            send(("rl", 1), ZS.at[0, pl.ds(0, OWN), :], RL.at[0], at_y(1))
            send(("rl", -1), ZS.at[0, pl.ds(OWN, OWN), :], RL.at[1], at_y(-1))
        elif d == 0:
            RES[...] = RES[...] + both
        else:
            k = 1 if d == 1 else 2
            free = OWN if d == 1 else 0
            ZS[k] = both.astype(BF16)
            PO[2 + (k - 1)] = both
            send(("rv", d), ZS.at[k, pl.ds(free, OWN), :], RV.at[k - 1, pl.ds(free, OWN), :], at_y(d))
    for d in (1, -1):
        k = 1 if d == 1 else 2
        held = OWN - (OWN if d == 1 else 0)
        recv(("rl", d), RL.at[k - 1])
        r = pl.ds(held, OWN)
        ZS[3, r, :] = (PO[2 + (k - 1), r, :] + RL[k - 1].astype(F32)).astype(BF16)
        send(("rw", d), ZS.at[3, r, :], RV.at[k - 1, r, :], at_y(d))
    for d in (1, -1):
        k = 1 if d == 1 else 2
        free = OWN if d == 1 else 0
        recv(("rv", d), RV.at[k - 1, pl.ds(free, OWN), :])
        recv(("rw", d), RV.at[k - 1, pl.ds(OWN - free, OWN), :])
    out_ref[...] = (RES[...] + RV[0].astype(F32) + RV[1].astype(F32)).astype(BF16)
    for d in started:
        d.wait_send()


def body(
    resid,
    query,
    keys,
    values,
    out_gate,
    in_gate,
    forget,
    doc_ids,
    head_gain,
    w_out,
    ffn_gain,
    w_gate,
    w_value,
    conv_taps,
    w_down,
):
    wd = w_down.T
    packed = jnp.concatenate(
        [
            w_gate,
            w_value[:, MAIN:],
            wd[:, MAIN:],
            jnp.zeros((HW, 32), BF16),
            w_value[:, :MAIN],
            wd[:, :MAIN],
        ],
        axis=1,
    )
    seg = doc_ids.astype(F32)[None]
    gates = jnp.concatenate([in_gate, forget, seg, jnp.zeros((3, TOK), F32)], axis=0)
    taps = jnp.pad(conv_taps, ((0, 0), (0, GW - conv_taps.shape[1])))
    vmem = pl.BlockSpec(memory_space=pltpu.VMEM)
    hbm = pl.BlockSpec(memory_space=pl.ANY)
    return pl.pallas_call(
        kernel,
        out_shape=jax.ShapeDtypeStruct((TOK, OWN), BF16),
        in_specs=[hbm, vmem, vmem, vmem, vmem, vmem, hbm, vmem, vmem, vmem, vmem],
        out_specs=vmem,
        scratch_shapes=[
            pltpu.VMEM((3072, LANES), BF16),
            pltpu.VMEM((TOK, 3072), BF16),
            pltpu.VMEM((TOK, 2048), BF16),
            pltpu.VMEM((2048, OWN), BF16),
            pltpu.VMEM((TOK, 256), BF16),
            pltpu.VMEM((TOK, 256), F32),
            pltpu.VMEM((TOK, 256), F32),
            pltpu.VMEM((TOK, 128), F32),
            pltpu.VMEM((200, 128), F32),
            pltpu.VMEM((4, 200, 128), F32),
            pltpu.VMEM((8, 8, TOK), F32),
            pltpu.VMEM((TOK, OWN), F32),
            pltpu.VMEM((TOK, GW), BF16),
            pltpu.VMEM((16, GW), BF16),
            pltpu.VMEM((TOK, GW), BF16),
            pltpu.VMEM((4, TOK, OWN), BF16),
            pltpu.VMEM((4, TOK, OWN), BF16),
            pltpu.VMEM((4, TOK, OWN), F32),
            pltpu.VMEM((4, TOK, OWN), BF16),
            pltpu.VMEM((2, OWN, OWN), BF16),
            pltpu.VMEM((2, TOK, OWN), BF16),
            pltpu.SemaphoreType.DMA((SEMS,)),
            pltpu.SemaphoreType.DMA((SEMS,)),
            pltpu.SemaphoreType.DMA((2,)),
        ],
        compiler_params=pltpu.CompilerParams(
            collective_id=0, has_side_effects=True, vmem_limit_bytes=63 * 1024 * 1024
        ),
    )(
        packed,
        query,
        keys,
        values,
        out_gate,
        gates,
        w_out,
        resid,
        head_gain[None],
        ffn_gain[None],
        taps,
    )


def solution(mesh):
    torus = Mesh(mesh.devices.reshape(4, 4, 4, 2), ("z", "x", "y", "c"))
    sp, tp = ("z", "x"), ("y", "c")
    placed = (
        P(sp, tp),
        P(sp, tp),
        P(sp, tp),
        P(sp, tp),
        P(sp, tp),
        P(tp, sp),
        P(tp, sp),
        P(sp),
        P(tp),
        P(tp, None),
        P(),
        P(sp, tp),
        P(sp, tp),
        P(None, tp),
        P(tp, sp),
    )
    return jax.shard_map(body, mesh=torus, in_specs=placed, out_specs=P(sp, tp), check_vma=False)
```

time: 441 us -> 166 us (0.38)
  waiting for transfers between devices: 161 us -> 0 us
  Pallas kernels: 0 us -> 155 us
  local copies, waits for them, and re-layouts: 80 us -> 10.1 us
  matrix products: 47.9 us -> 0 us
  other arithmetic: 42.4 us -> 0.67 us
  loops' own time: 38.2 us -> 0 us
  between operations: 37.6 us -> 0.1 us
  blocking collectives: 27.3 us -> 0 us
    pallas_call x0 -> x1, Pallas kernels: none -> 155 us  [body(): pl.pallas_call(kernel, out_shape=jax.ShapeDtypeStruct((TOK, OWN), BF16),...]
    psum x1 -> x0, waiting for transfers between devices: 109 us -> none  [body(): full_rows = lax.psum(term + placed, 'tp')]
    dot_general x7 -> x0, matrix products: 47.9 us -> none  [the longest x1 18.2 us: body(): value = jnp.dot(normed_rows, pieces[1], preferred_element_type=jnp.float32)]
    unnamed x5 -> x0, waiting for transfers between devices: 39.4 us -> none
    another operation x1 -> x0, loops' own time: 38.2 us -> none  [body(): local_end, before = lax.scan(advance, empty_state(heads, DH), elements)]
    dynamic_update_slice x48 -> x0, local copies, waits for them, and re-layouts: 33.1 us -> none  [body(): local_end, before = lax.scan(advance, empty_state(heads, DH), elements)]
    all_gather x2 -> x0, blocking collectives: 27.3 us -> none  [collected_together(): both, at, found = (lax.all_gather(jnp.concatenate(lines), axis), 0, {})]
    dynamic_slice x24 -> x0, local copies, waits for them, and re-layouts: 13.8 us -> none  [body(): local_end, before = lax.scan(advance, empty_state(heads, DH), elements)]
  transfers between devices with their start and end apart: 5 -> 0, of which waited for: 4 -> 0; matrix products, arithmetic and copies ran while one was open for 9% -> 0% of each run, Pallas kernels for 0% -> 0%
where the time goes in v1:
time: 166 us
  Pallas kernels  155 us (93%)
  local copies, waits for them, and re-layouts  10.1 us (6%)
    pallas_call x1, Pallas kernels, body(): pl.pallas_call(kernel, out_shape=jax.ShapeDtypeStruct((TOK, OWN), BF16),...  155 us
    unnamed x23, local copies, waits for them, and re-layouts  5.73 us

profile of v1, /device:TPU:0, one launch (start us, length us, event | category | flops | bytes accessed | tf_op | source)
XLA Modules:
  0.0 165.9 jit_solution(2058789058856228178)
XLA Ops:
  0.0 0.0 slice-start
  0.0 0.0 slice-start.1
  0.0 0.0 copy-start
  0.0 1.1 slice.17
  1.1 0.8 slice.16
  1.9 0.0 slice-done
  1.9 0.0 slice-done.1
  1.9 0.0 copy-done
  2.0 0.0 copy-start.1
  2.0 0.0 copy-start.2
  2.0 1.8 %concatenate.6.pk = bf16[192,3200]{1,0:T(8,128)(2,1)} concatenate(bf16[192,1056]{1,0:T(8,128)(2,1)S(1)} %copy-done, bf16[192,32]{1,0:T(8,128)(2,1)S(1)} %slice-done.1, bf16[192,32]{1,0:T(8,128)(2,1)S(1)} %slice.16, bf16[192,32]{1,0:T(8,128)(2,1)S(1)} %broadcast_in_dim.15, bf16[192,1024]{1,0:T(8,128)(2,1)S(1)} %slice-done, bf16[192,1024]{1,0:T(8,128)(2,1)S(1)} %slice.17), dimensions={1} | concatenate | bytes 2457600 | tf_op jit(solution)/shard_map/concatenate | solution.py:524
  3.8 0.0 copy-done.1
  3.8 0.0 copy-start.3
  3.8 0.0 copy-start.4
  3.8 0.0 copy-start.6
  3.8 0.0 copy-start.7
  3.8 0.9 copy.16.q_ref
  4.7 0.0 copy-done.2
  4.7 1.0 copy.17.k_ref
  5.7 0.0 copy-done.3
  5.7 0.9 copy.18.v_ref
  6.6 0.0 copy-done.4
  6.6 0.9 copy.19.og_ref
  7.5 0.0 copy-done.8
  7.6 0.1 pad.8.clone
  7.6 0.0 copy-done.6
  7.6 0.0 copy-done.7
  7.6 0.7 maximum_maximum_fusion.gates_ref
  8.3 0.0 copy-done.5
  8.3 0.6 pad.4.taps_ref
  8.9 155.0 %shard_map.145 = bf16[768,384]{1,0:T(8,128)(2,1)} custom-call(bf16[192,3200]{1,0:T(8,128)(2,1)} %concatenate.6.pk, bf16[768,192]{1,0:T(8,128)(2,1)} %copy.16.q_ref, bf16[768,192]{1,0:T(8,128)(2,1)} %copy.17.k_ref, bf16[768,192]{1,0:T(8,128)(2,1)} %copy.18.v_ref, bf16[768,192]{1,0:T(8,128)(2,1)} %copy.19.og_ref, f32[8,768]{1,0:T(8,128)} %maximum_maximum_fusion.gates_ref, ...), custom_call_target="tpu_custom_call" | custom-call | tf_op jit(solution)/shard_map/pallas_call | solution.py:540
  164.0 1.9 %copy.21 = bf16[768,384]{1,0:T(8,128)(2,1)} copy(bf16[768,384]{1,0:T(8,128)(2,1)} %shard_map.145) | data formatting | bytes 1179648
  (6 shorter events, 0.0 us)
Async XLA Ops:
  0.0 1.9 %slice-start = ((bf16[192,1056]{1,0:T(8,128)(2,1)}), bf16[192,1024]{1,0:T(8,128)(2,1)S(1)}, s32[]{:S(2)}) async-start(bf16[192,1056]{1,0:T(8,128)(2,1)} %param.27), calls=%async_computation | async-start | bytes 786432 | tf_op jit(solution)/shard_map/slice | solution.py:530
  0.0 1.9 %slice-start.1 = ((bf16[192,1056]{1,0:T(8,128)(2,1)}), bf16[192,32]{1,0:T(8,128)(2,1)S(1)}, s32[]{:S(2)}) async-start(bf16[192,1056]{1,0:T(8,128)(2,1)} %param.27), calls=%async_computation.1 | async-start | bytes 98304 | tf_op jit(solution)/shard_map/slice | solution.py:527
  0.0 1.9 %copy-start = (bf16[192,1056]{1,0:T(8,128)(2,1)S(1)}, bf16[192,1056]{1,0:T(8,128)(2,1)}, u32[]{:S(2)}) copy-start(bf16[192,1056]{1,0:T(8,128)(2,1)} %param.26) | copy-start | bytes 1216516
  2.0 1.8 %copy-start.1 = (bf16[768,192]{0,1:T(8,128)(2,1)S(1)}, bf16[768,192]{0,1:T(8,128)(2,1)}, u32[]{:S(2)}) copy-start(bf16[768,192]{0,1:T(8,128)(2,1)} %param.16) | copy-start | bytes 884740
  2.0 2.7 %copy-start.2 = (bf16[768,192]{0,1:T(8,128)(2,1)S(1)}, bf16[768,192]{0,1:T(8,128)(2,1)}, u32[]{:S(2)}) copy-start(bf16[768,192]{0,1:T(8,128)(2,1)} %param.17) | copy-start | bytes 884740
  3.8 1.9 %copy-start.3 = (bf16[768,192]{0,1:T(8,128)(2,1)S(1)}, bf16[768,192]{0,1:T(8,128)(2,1)}, u32[]{:S(2)}) copy-start(bf16[768,192]{0,1:T(8,128)(2,1)} %param.18) | copy-start | bytes 884740
  3.8 2.8 %copy-start.4 = (bf16[768,192]{0,1:T(8,128)(2,1)S(1)}, bf16[768,192]{0,1:T(8,128)(2,1)}, u32[]{:S(2)}) copy-start(bf16[768,192]{0,1:T(8,128)(2,1)} %param.19) | copy-start | bytes 884740
  3.8 3.8 %copy-start.8 = (s32[768]{0:T(1024)S(1)}, s32[768]{0:T(1024)}, u32[]{:S(2)}) copy-start(s32[768]{0:T(1024)} %param.22) | copy-start | bytes 9220
  3.8 3.9 %copy-start.6 = (f32[2,768]{1,0:T(2,128)S(1)}, f32[2,768]{1,0:T(2,128)}, u32[]{:S(2)}) copy-start(f32[2,768]{1,0:T(2,128)} %param.21) | copy-start | bytes 18436
  3.8 3.9 %copy-start.7 = (f32[2,768]{1,0:T(2,128)S(1)}, f32[2,768]{1,0:T(2,128)}, u32[]{:S(2)}) copy-start(f32[2,768]{1,0:T(2,128)} %param.20) | copy-start | bytes 18436
  4.7 3.6 %copy-start.5 = (f32[3,1056]{1,0:T(4,128)S(1)}, f32[3,1056]{1,0:T(4,128)}, u32[]{:S(2)}) copy-start(f32[3,1056]{1,0:T(4,128)} %param.28) | copy-start | bytes 38020

commit v2 on v1

v2 whole, which is shorter than its diff:
```python
import jax
import jax.numpy as jnp
from jax import lax
from jax.experimental import pallas as pl
from jax.experimental.pallas import tpu as pltpu
from jax.sharding import Mesh
from jax.sharding import PartitionSpec as P

MESH = pl.DeviceIdType.MESH
F32 = jnp.float32
BF16 = jnp.bfloat16
ABSENT = -1e30
DH = 96
TOK = 768
OWN = 384
HW = 192
MAIN = 1024
GW = 1152
LANES = 2176
ONE = 128
TWO = 64
EPS = 1e-6
SEMS = 224
scope = jax.named_scope


def mod4(v):
    return lax.rem(v + 8, 4)


def dot(a, b, **kw):
    return lax.dot_general(a, b, (((1,), (0,)), ((), ())), preferred_element_type=F32, **kw)


def dot_t(a, b, **kw):
    return lax.dot_general(a, b, (((1,), (1,)), ((), ())), preferred_element_type=F32, **kw)


def dot_c(a, b, **kw):
    return lax.dot_general(a, b, (((0,), (0,)), ((), ())), preferred_element_type=F32, **kw)


def kernel(
    wg_ref,
    wv_ref,
    wd_ref,
    q_hbm,
    k_hbm,
    v_hbm,
    og_hbm,
    wo_ref,
    resid_hbm,
    ig_ref,
    fg_ref,
    seg_ref,
    hg_ref,
    gain_ref,
    taps_ref,
    out_ref,
    W,
    WD1,
    WD2,
    TL,
    X,
    MIX,
    WO,
    WOT,
    QT,
    KT,
    VT,
    OG,
    RB,
    OI,
    NF,
    ST,
    SR,
    SS,
    RES,
    ACC,
    GT,
    EDGE,
    HD,
    SP,
    RP,
    PO,
    ZS,
    RL,
    RV,
    ssem,
    rsem,
    lsem,
):
    z, x = lax.axis_index("z"), lax.axis_index("x")
    y, c = lax.axis_index("y"), lax.axis_index("c")
    sp = z * 4 + x
    tp = y * 2 + c
    o = 1 - c
    table = {}
    started = []

    def slot(key):
        return table.setdefault(key, len(table))

    def send(key, src, dst, dev):
        i = slot(key)
        d = pltpu.make_async_remote_copy(
            src_ref=src,
            dst_ref=dst,
            send_sem=ssem.at[i],
            recv_sem=rsem.at[i],
            device_id=dev,
            device_id_type=MESH,
        )
        d.start()
        started.append(d)

    partner = (z, x, y, o)

    def recv(key, dst):
        i = slot(key)
        pltpu.make_async_remote_copy(
            src_ref=dst,
            dst_ref=dst,
            send_sem=ssem.at[i],
            recv_sem=rsem.at[i],
            device_id=partner,
            device_id_type=MESH,
        ).wait_recv()

    def at_sp(n):
        s = lax.rem(sp + n + 16, 16)
        return (s // 4, lax.rem(s, 4), y, c)

    def at_x(d):
        return (z, mod4(x + d), y, c)

    def at_z(d):
        return (mod4(z + d), x, y, c)

    def at_y(d):
        return (z, x, mod4(y + d), c)

    def at_tp(n):
        t = lax.rem(tp + n, 8)
        return (z, x, t // 2, lax.rem(t, 2))

    peers = [at_x(1), at_x(-1), at_z(1), at_z(-1)]
    peers += [at_tp(n) for n in range(1, 8)]
    peers += [at_sp(n) for n in (1, 2, 3, -1, -2, -3)]
    barrier = pltpu.get_barrier_semaphore()
    for dev in peers:
        pl.semaphore_signal(barrier, inc=1, device_id=dev, device_id_type=MESH)

    local = []

    def bring(src, dst):
        d = pltpu.make_async_copy(src, dst, lsem.at[len(local)])
        d.start()
        local.append(d)

    own_w = pl.ds(pl.multiple_of(sp * HW, 16), HW)
    bring(wg_ref.at[:, 0:MAIN], W.at[own_w, 0:MAIN])
    bring(wv_ref.at[:, 0:MAIN], W.at[own_w, GW:LANES])
    for n, ref in enumerate((wg_ref, wv_ref, wd_ref)):
        bring(ref.at[:, MAIN : MAIN + 32], TL.at[n])
    bring(k_hbm, KT)
    bring(v_hbm, VT)
    bring(q_hbm, QT)
    bring(og_hbm, OG)
    bring(wd_ref.at[0:ONE, 0:MAIN], WD1.at[pl.ds(pl.multiple_of(sp * ONE, 16), ONE), :])
    bring(wd_ref.at[ONE:HW, 0:MAIN], WD2.at[pl.ds(pl.multiple_of(sp * TWO, 16), TWO), :])
    bring(resid_hbm, RB)
    bring(
        wo_ref.at[:, pl.ds(pl.multiple_of(tp * OWN, 128), OWN)],
        WO.at[pl.ds(pl.multiple_of(tp * HW, 16), HW), :],
    )

    def stage(name, ref, stride, rows, lanes, cut, first):
        x_first = first == "x"
        prim = at_x if x_first else at_z
        secd = at_z if x_first else at_x
        steps = (0, -1, 1, 2)

        def place(dp, ds, half=None):
            zz, xx = (mod4(z + ds), mod4(x + dp)) if x_first else (mod4(z + dp), mod4(x + ds))
            r0, nr = rows
            if half is not None:
                r0, nr = r0 + (cut[0] if half else 0), cut[half]
            row = pl.multiple_of((zz * 4 + xx) * stride + r0, 16)
            return ref.at[pl.ds(row, nr), pl.ds(lanes[0], lanes[1])]

        def primary():
            for d in (1, -1):
                send((name, "p", d), place(0, 0), place(0, 0), prim(d))

        def second(m):
            p = place(steps[m], 0)
            for d in (1, -1):
                send((name, "s", d, m), p, p, secd(d))

        def relay():
            for d in (1, -1):
                recv((name, "p", d), place(-d, 0))
                p = place(-d, 0, 0 if d == 1 else 1)
                send((name, "pf", d), p, p, prim(d))

        def across(m):
            for d in (1, -1):
                recv((name, "s", d, m), place(steps[m], -d))
                p = place(steps[m], -d, 0 if d == 1 else 1)
                send((name, "sf", d, m), p, p, secd(d))

        def far():
            for d in (1, -1):
                recv((name, "pf", d), place(2, 0, 0 if d == 1 else 1))
            second(3)

        def done():
            for m in range(4):
                for d in (1, -1):
                    recv((name, "sf", d, m), place(steps[m], 2, 0 if d == 1 else 1))

        return primary, second, relay, across, far, done

    def run(stages, what, *args):
        k = ("primary", "second", "relay", "across", "far", "done").index(what)
        for st in stages:
            st[k](*args)

    gv = (
        stage("g", W, HW, (0, HW), (0, GW), (96, 96), "x"),
        stage("v", W, HW, (0, HW), (GW, MAIN), (96, 96), "z"),
    )
    d1 = (
        stage("d1a", WD1, ONE, (0, 48), (0, MAIN), (32, 16), "x"),
        stage("d1b", WD1, ONE, (48, 80), (0, MAIN), (48, 32), "z"),
    )
    d2 = (
        stage("d2a", WD2, TWO, (0, 32), (0, MAIN), (16, 16), "x"),
        stage("d2b", WD2, TWO, (32, 32), (0, MAIN), (16, 16), "z"),
    )

    def over_tp(name, blk):
        def g0():
            b = blk(y, c)
            for d in (1, -1):
                send((name, "y", d), b, b, at_y(d))
            send((name, "o"), b, b, partner)

        def g1():
            for d in (1, -1):
                src = mod4(y - d)
                recv((name, "y", d), blk(src, c))
                h = blk(src, c, 0 if d == 1 else 1)
                send((name, "f", d), h, h, at_y(d))
            for d in (1, -1):
                src = mod4(y - d)
                send((name, "of", d), blk(src, c), blk(src, c), partner)

        def g2():
            far = mod4(y + 2)
            for d in (1, -1):
                h = blk(far, c, 0 if d == 1 else 1)
                recv((name, "f", d), h)
                send((name, "oh", d), h, h, partner)

        def g3():
            far = mod4(y + 2)
            recv((name, "o"), blk(y, o))
            for d in (1, -1):
                recv((name, "of", d), blk(mod4(y - d), o))
                recv((name, "oh", d), blk(far, o, 0 if d == 1 else 1))

        return g0, g1, g2, g3

    def mix_block(yy, cc, half=None):
        r0, nr = (0, HW) if half is None else (half * DH, DH)
        return MIX.at[pl.ds(pl.multiple_of((yy * 2 + cc) * HW + r0, 16), nr), :]

    def x_block(yy, cc, half=None):
        rows = slice(None) if half is None else pl.ds(half * OWN, OWN)
        return X.at[rows, pl.ds(pl.multiple_of((yy * 2 + cc) * OWN, 128), OWN)]

    mix_g = over_tp("m", mix_block)
    x_g = over_tp("x", x_block)

    for d in local[:5]:
        d.wait()
    tails = jnp.concatenate([TL[0], TL[1], TL[2], jnp.zeros((HW, 32), BF16)], axis=1)
    W[own_w, MAIN:GW] = tails
    with scope("barrier"):
        pl.semaphore_wait(barrier, len(peers))
    run(gv[1:], "primary")
    run(gv[:1], "primary")
    for n in range(1, 8):
        t = lax.rem(tp + n, 8)
        src = wo_ref.at[:, pl.ds(pl.multiple_of(t * OWN, 128), OWN)]
        dst = WO.at[pl.ds(pl.multiple_of(tp * HW, 16), HW), :]
        send(("w", n), src, dst, at_tp(n))

    lane = lax.broadcasted_iota(jnp.int32, (8, TOK), 1)
    row8 = lax.broadcasted_iota(jnp.int32, (8, TOK), 0)
    seg = seg_ref[...].astype(F32)
    fg = jnp.where(row8 == 0, fg_ref[0:1], fg_ref[1:2])
    e = jnp.exp(-jnp.abs(fg))
    log1p = jnp.where(e < 1e-2, e * (1.0 - e * (0.5 - e * (1.0 / 3.0))), jnp.log(1.0 + e))
    cum = jnp.minimum(fg, 0.0) - log1p
    shift = 1
    while shift < TOK:
        cum = cum + jnp.where(lane >= shift, pltpu.roll(cum, shift, 1), 0.0)
        shift *= 2
    b = [ig_ref[h : h + 1] - cum[h : h + 1] for h in range(2)]
    end = [cum[h : h + 1, TOK - 1 :] for h in range(2)]
    first, last, second_last = seg[:, :1], seg[:, TOK - 1 :], seg[:, TOK - 2 : TOK - 1]
    for d in local[5:9]:
        d.wait()
    ST[...] = jnp.zeros_like(ST)
    peak = []
    for h in range(2):
        hs = slice(h * DH, h * DH + DH)
        top = jnp.max(jnp.where(seg == last, b[h], ABSENT), axis=1, keepdims=True)
        peak.append(top)
        w = jnp.where(seg == last, jnp.exp(jnp.minimum(b[h] - top, 0.0)), 0.0) * DH**-0.5
        ST[hs, 0:DH] = dot_t(VT[hs, :], (KT[hs, :].astype(F32) * w).astype(BF16))
    meta_row = lax.broadcasted_iota(jnp.int32, (8, 128), 0)
    meta = jnp.zeros((8, 128), F32)
    for n, value in enumerate((end[0] + peak[0], end[1] + peak[1], end[0], end[1], first, last, second_last)):
        meta = jnp.where(meta_row == n, value, meta)
    ST[HW : HW + 8, :] = meta
    for n in range(1, 5):
        send(("st", n), ST, SR.at[n - 1], at_sp(n))
    run(gv, "second", 0)

    rows = jnp.where(row8 == 0, b[0], jnp.where(row8 == 1, b[1], seg))
    cols = jnp.transpose(jnp.concatenate([rows, jnp.zeros((120, TOK), F32)], axis=0))
    seg_c = cols[:, 2:3]
    tops = [[], []]
    for i in range(3):
        t0, ns = i * 256, (i + 1) * 256
        ts = slice(t0, t0 + 256)
        s_at = lax.broadcasted_iota(jnp.int32, (ns, 256), 0)
        t_at = lax.broadcasted_iota(jnp.int32, (ns, 256), 1) + t0
        mask = (seg_c[:ns] == seg[:, ts]) & (s_at <= t_at)
        for h in range(2):
            hs = slice(h * DH, h * DH + DH)
            masked = jnp.where(mask, cols[:ns, h : h + 1], ABSENT)
            top = jnp.max(masked, axis=0, keepdims=True)
            scores = dot_c(KT[hs, 0:ns], QT[hs, ts]) * (jnp.exp(masked - top) * DH**-0.5)
            OI[hs, ts] = dot(VT[hs, 0:ns], scores.astype(BF16))
            tops[h].append(top)

    with scope("relay"):
        run(gv, "relay")
        run(gv, "second", 1)
        run(gv, "second", 2)

    dec = [jnp.zeros((1, 128), F32)] * 2
    cand = [[], []]
    first_l = jnp.broadcast_to(first, (1, 128))
    with scope("state"):
        for n in range(1, 5):
            recv(("st", n), SR.at[n - 1])
    for n in range(1, 5):
        m = SR[n - 1, HW : HW + 8, :]
        valid = (m[5:6] == first_l) & (sp >= n)
        for h in range(2):
            cand[h].append(jnp.where(valid, m[h : h + 1] + dec[h], ABSENT))
            dec[h] = dec[h] + m[2 + h : 3 + h]
    gain_at = lax.broadcasted_iota(jnp.int32, (HW, HW), 0) == lax.broadcasted_iota(jnp.int32, (HW, HW), 1)
    gain_c = jnp.sum(jnp.where(gain_at, hg_ref[...], 0.0), axis=1, keepdims=True)
    for h in range(2):
        hs = slice(h * DH, h * DH + DH)
        pin = jnp.maximum(
            jnp.maximum(cand[h][0], cand[h][1]), jnp.maximum(cand[h][2], cand[h][3])
        )
        state = jnp.zeros((DH, 128), F32)
        for n in range(4):
            state = state + jnp.exp(cand[h][n] - pin) * SR[n, hs, :]
        inter = dot(state[:, 0:DH].astype(BF16), QT[hs, :])
        m_in = jnp.concatenate(tops[h], axis=1)
        m_pin = jnp.where(seg == first, pin[:, :1], ABSENT)
        m_all = jnp.maximum(m_in, m_pin)
        memory = jnp.exp(m_in - m_all) * OI[hs, :] + jnp.exp(m_pin - m_all) * inter
        mean = jnp.sum(memory * memory, axis=0, keepdims=True) * (1.0 / DH)
        mix = memory * lax.rsqrt(mean + 1.0) * gain_c[hs] * jax.nn.sigmoid(OG[hs, :].astype(F32))
        MIX[pl.ds(pl.multiple_of(tp * HW + h * DH, 16), DH), :] = mix.astype(BF16)
    with scope("mix0"):
        mix_g[0]()
    with scope("across0"):
        run(gv, "across", 0)

    before = SR[0, HW : HW + 8, :]
    there = sp >= 1
    last_before = jnp.where(there, before[5:6, :1], -1.0)
    second_before = jnp.where(there, before[6:7, :1], -1.0)
    seg8 = jnp.broadcast_to(seg, (8, TOK))
    one_back = jnp.where(lane == 0, last_before, pltpu.roll(seg8, 1, 1))
    two_back = jnp.where(
        lane == 0, second_before, jnp.where(lane == 1, last_before, pltpu.roll(seg8, 2, 1))
    )
    flags = jnp.where(
        row8 == 0, jnp.where(one_back == seg, 1.0, 0.0), jnp.where(two_back == seg, 1.0, 0.0)
    )
    NF[...] = jnp.transpose(jnp.concatenate([flags, jnp.zeros((120, TOK), F32)], axis=0))
    with scope("wo"):
        for d in local[9:]:
            d.wait()
        for n in range(1, 8):
            t = lax.rem(tp + 8 - n, 8)
            recv(("w", n), WO.at[pl.ds(pl.multiple_of(t * HW, 16), HW), :])
        WOT[...] = jnp.transpose(WO[...])

    with scope("mix1"):
        mix_g[1]()
    with scope("far"):
        run(gv, "far")
    with scope("mix2"):
        mix_g[2]()
    with scope("mix3"):
        mix_g[3]()

    gain = gain_ref[:, pl.ds(pl.multiple_of(tp * OWN, 128), OWN)]
    res = RB[...].astype(F32) + jnp.transpose(dot(WOT[...], MIX[...]))
    RES[...] = res
    X[:, pl.ds(pl.multiple_of(tp * OWN, 128), OWN)] = (res * gain).astype(BF16)
    x_g[0]()
    SS[tp] = dot_t(jnp.ones((8, OWN), F32), res * res, precision=lax.Precision.HIGHEST)
    for n in range(1, 8):
        send(("q", n), SS.at[tp], SS.at[tp], at_tp(n))
    with scope("across1"):
        run(gv, "across", 1)
    with scope("across2"):
        run(gv, "across", 2)
    with scope("x1"):
        x_g[1]()
    with scope("x2"):
        x_g[2]()
    with scope("x3"):
        x_g[3]()
    with scope("across3"):
        run(gv, "across", 3)
        run(d1, "primary")
        run(d1, "second", 0)
    with scope("sq"):
        total = SS[tp]
        for n in range(1, 8):
            t = lax.rem(tp + 8 - n, 8)
            recv(("q", n), SS.at[t])
            total = total + SS[t]
    scale_row = lax.rsqrt(total * (1.0 / 3072.0) + EPS)
    NF[:, 2:3] = jnp.transpose(jnp.concatenate([scale_row, jnp.zeros((120, TOK), F32)], axis=0))[:, 0:1]

    def tile256(n, at):
        return pl.ds(pl.multiple_of(n * 256 + at, 128), 256)

    def by_row(lanes, steps):
        acc = None
        for d in steps:
            k = pl.ds(pl.multiple_of(mod4(z + d) * 768, 128), 768)
            part = dot(X[:, k], W[k, lanes])
            acc = part if acc is None else acc + part
        return acc

    def by_pair(lanes, which):
        acc = None
        for zz in range(4):
            k = pl.ds(pl.multiple_of(zz * 768 + which * OWN, 128), OWN)
            part = dot(X[:, k], W[k, lanes])
            acc = part if acc is None else acc + part
        return acc

    here = x // 2
    with scope("partial"):

        def early(n, _):
            ACC[:, tile256(n, 0)] = by_row(tile256(n, 0), (0, 1, -1))
            ACC[:, tile256(n, GW)] = by_pair(tile256(n, GW), here)
            return 0

        lax.fori_loop(0, 4, early, 0)
        ACC[:, MAIN:GW] = by_row(slice(MAIN, GW), (0, 1, -1))

    with scope("done"):
        run(gv, "done")
    with scope("d1relay"):
        run(d1, "relay")
        run(d1, "second", 1)
        run(d1, "second", 2)
    scale = NF[:, 2:3]
    with scope("gate"):

        def gate_tile(n, _):
            l = tile256(n, 0)
            GT[:, l] = ((ACC[:, l] + by_row(l, (2,))) * scale).astype(BF16)
            return 0

        lax.fori_loop(0, 4, gate_tile, 0)
        l = slice(MAIN, GW)
        GT[:, l] = ((ACC[:, l] + by_row(l, (2,))) * scale).astype(BF16)
    send(("e",), GT.at[TOK - 16 : TOK, :], EDGE, at_sp(1))
    with scope("d1across0"):
        run(d1, "across", 0)

    def hidden_of(lanes, width, taps, value):
        g = GT[:, lanes].astype(F32)
        edge = EDGE[:, lanes].astype(F32)
        t_at = lax.broadcasted_iota(jnp.int32, (TOK, width), 0)
        near = NF[:, 0:1] > 0.5
        far = NF[:, 1:2] > 0.5
        g1 = jnp.where(t_at == 0, edge[15:16], pltpu.roll(g, 1, 0))
        g2 = jnp.where(
            t_at == 0, edge[14:15], jnp.where(t_at == 1, edge[15:16], pltpu.roll(g, 2, 0))
        )
        conv = taps[2:3] * g + taps[1:2] * jnp.where(near, g1, 0.0) + taps[0:1] * jnp.where(far, g2, 0.0)
        return conv / (1.0 + jnp.exp(-conv)) * value

    def value_sum(n, _):
        l = tile256(n, GW)
        ACC[:, l] = ACC[:, l] + by_pair(l, 1 - here)
        return 0

    with scope("value"):
        lax.fori_loop(0, 4, value_sum, 0)
    with scope("d1far"):
        run(d1, "far")
    with scope("edge"):
        recv(("e",), EDGE)

    with scope("hidden"):

        def hidden_tile(n, _):
            value = (ACC[:, tile256(n, GW)] * scale).astype(BF16).astype(F32)
            l = tile256(n, 0)
            HD[:, l] = hidden_of(l, 256, taps_ref[:, l], value).astype(BF16)
            return 0

        lax.fori_loop(0, 4, hidden_tile, 0)
        tail = slice(MAIN, GW)
        taps_tail = jnp.concatenate([taps_ref[:, MAIN : MAIN + 32], jnp.zeros((3, 96), F32)], axis=1)
        value_tail = pltpu.roll(GT[:, tail].astype(F32), 96, 1)
        HD[:, tail] = pltpu.roll(hidden_of(tail, 128, taps_tail, value_tail), 64, 1).astype(BF16)
    with scope("d1rest"):
        run(d1, "across", 1)
        run(d1, "across", 2)
        run(d2, "primary")
        run(d2, "second", 0)
        run(d1, "across", 3)
        run(d2, "relay")
        run(d2, "second", 1)
        run(d2, "second", 2)
        run(d1, "done")

    def partial(p, yy, cc):
        j = yy * 2 + cc
        size = ONE if p == 0 else TWO
        ref = WD1 if p == 0 else WD2
        r = pl.ds(pl.multiple_of(j * 2 * size, 128), 2 * size)
        ends = []
        for k in range(2):
            at = (j * 2 + k) * HW + (0 if p == 0 else ONE)
            ends.append(W[pl.ds(pl.multiple_of(at, 16), size), MAIN:GW])
        return dot_t(HD[:, 0:MAIN], ref[r, :]) + dot_t(HD[:, MAIN:GW], jnp.concatenate(ends, axis=0))

    order = (2, 1, -1, 0)
    lanes_of = (pl.ds(0, 2 * ONE), pl.ds(2 * ONE, 2 * TWO))

    def reduce_part(p, between):
        l = lanes_of[p]

        def give(n):
            yy = mod4(y + order[n])
            SP[n, :, l] = partial(p, yy, o).astype(BF16)
            send(("sp", p, n), SP.at[n, :, l], RP.at[n, :, l], partner)

        give(0)
        for n, d in enumerate(order):
            if n < 3:
                give(n + 1)
            PO[n, :, l] = partial(p, mod4(y + d), c)
            with scope("sp%d" % n):
                recv(("sp", p, n), RP.at[n, :, l])
            both = PO[n, :, l] + RP[n, :, l].astype(F32)
            if d == 2:
                ZS[0, :, l] = both.astype(BF16)
                send(("rl", p, 1), ZS.at[0, pl.ds(0, OWN), l], RL.at[0, :, l], at_y(1))
                send(("rl", p, -1), ZS.at[0, pl.ds(OWN, OWN), l], RL.at[1, :, l], at_y(-1))
            else:
                PO[n, :, l] = both
                if d != 0:
                    r = pl.ds(OWN if d == 1 else 0, OWN)
                    ZS[n, r, l] = PO[n, r, l].astype(BF16)
                    send(("rv", p, d), ZS.at[n, r, l], RV.at[n - 1, r, l], at_y(d))
            between[n]()
        for n, d in ((1, 1), (2, -1)):
            r = pl.ds(0 if d == 1 else OWN, OWN)
            with scope("rl"):
                recv(("rl", p, d), RL.at[n - 1, :, l])
            ZS[n, r, l] = (PO[n, r, l] + RL[n - 1, :, l].astype(F32)).astype(BF16)
            send(("rw", p, d), ZS.at[n, r, l], RV.at[n - 1, r, l], at_y(d))

    def collect(p):
        l = lanes_of[p]
        for n, d in ((1, 1), (2, -1)):
            with scope("rv"):
                recv(("rv", p, d), RV.at[n - 1, pl.ds(OWN if d == 1 else 0, OWN), l])
                recv(("rw", p, d), RV.at[n - 1, pl.ds(0 if d == 1 else OWN, OWN), l])
        return PO[3, :, l] + RV[0, :, l].astype(F32) + RV[1, :, l].astype(F32)

    nothing = lambda: None
    with scope("reduce1"):
        reduce_part(
            0,
            [
                lambda: run(d2, "across", 0),
                lambda: run(d2, "far"),
                lambda: run(d2, "across", 1),
                lambda: run(d2, "across", 2),
            ],
        )
    with scope("d2rest"):
        run(d2, "across", 3)
        run(d2, "done")
    with scope("reduce2"):
        reduce_part(1, [nothing] * 4)
    with scope("final"):
        wide = collect(0)
        slim = collect(1)
        turned = pltpu.roll(wide[:, ONE:], 64, 1)
        low = lax.broadcasted_iota(jnp.int32, (TOK, 128), 1) < 64
        out_ref[:, 0:128] = (RES[:, 0:128] + wide[:, :ONE]).astype(BF16)
        out_ref[:, 128:256] = (RES[:, 128:256] + jnp.where(low, slim, turned)).astype(BF16)
        out_ref[:, 256:384] = (RES[:, 256:384] + jnp.where(low, turned, slim)).astype(BF16)
        for d in started:
            d.wait_send()


def body(
    resid,
    query,
    keys,
    values,
    out_gate,
    in_gate,
    forget,
    doc_ids,
    head_gain,
    w_out,
    ffn_gain,
    w_gate,
    w_value,
    conv_taps,
    w_down,
):
    vmem = pl.BlockSpec(memory_space=pltpu.VMEM)
    hbm = pl.BlockSpec(memory_space=pl.ANY)
    return pl.pallas_call(
        kernel,
        out_shape=jax.ShapeDtypeStruct((TOK, OWN), BF16),
        in_specs=[hbm] * 9 + [vmem] * 6,
        out_specs=vmem,
        scratch_shapes=[
            pltpu.VMEM((3072, LANES), BF16),
            pltpu.VMEM((16 * ONE, MAIN), BF16),
            pltpu.VMEM((16 * TWO, MAIN), BF16),
            pltpu.VMEM((3, HW, 32), BF16),
            pltpu.VMEM((TOK, 3072), BF16),
            pltpu.VMEM((1536, TOK), BF16),
            pltpu.VMEM((1536, OWN), BF16),
            pltpu.VMEM((OWN, 1536), BF16),
            pltpu.VMEM((HW, TOK), BF16),
            pltpu.VMEM((HW, TOK), BF16),
            pltpu.VMEM((HW, TOK), BF16),
            pltpu.VMEM((HW, TOK), BF16),
            pltpu.VMEM((TOK, OWN), BF16),
            pltpu.VMEM((HW, TOK), F32),
            pltpu.VMEM((TOK, 128), F32),
            pltpu.VMEM((200, 128), F32),
            pltpu.VMEM((4, 200, 128), F32),
            pltpu.VMEM((8, 8, TOK), F32),
            pltpu.VMEM((TOK, OWN), F32),
            pltpu.VMEM((TOK, LANES), F32),
            pltpu.VMEM((TOK, GW), BF16),
            pltpu.VMEM((16, GW), BF16),
            pltpu.VMEM((TOK, GW), BF16),
            pltpu.VMEM((4, TOK, OWN), BF16),
            pltpu.VMEM((4, TOK, OWN), BF16),
            pltpu.VMEM((4, TOK, OWN), F32),
            pltpu.VMEM((3, TOK, OWN), BF16),
            pltpu.VMEM((2, OWN, OWN), BF16),
            pltpu.VMEM((2, TOK, OWN), BF16),
            pltpu.SemaphoreType.DMA((SEMS,)),
            pltpu.SemaphoreType.DMA((SEMS,)),
            pltpu.SemaphoreType.DMA((16,)),
        ],
        compiler_params=pltpu.CompilerParams(
            collective_id=0, has_side_effects=True, vmem_limit_bytes=63 * 1024 * 1024
        ),
    )(
        w_gate,
        w_value,
        w_down.T,
        query.T,
        keys.T,
        values.T,
        out_gate.T,
        w_out,
        resid,
        in_gate,
        forget,
        doc_ids[None],
        head_gain[None],
        ffn_gain[None],
        conv_taps,
    )


def solution(mesh):
    torus = Mesh(mesh.devices.reshape(4, 4, 4, 2), ("z", "x", "y", "c"))
    sp, tp = ("z", "x"), ("y", "c")
    placed = (
        P(sp, tp),
        P(sp, tp),
        P(sp, tp),
        P(sp, tp),
        P(sp, tp),
        P(tp, sp),
        P(tp, sp),
        P(sp),
        P(tp),
        P(tp, None),
        P(),
        P(sp, tp),
        P(sp, tp),
        P(None, tp),
        P(tp, sp),
    )
    return jax.shard_map(body, mesh=torus, in_specs=placed, out_specs=P(sp, tp), check_vma=False)
```

time: 166 us -> 151 us (0.910)
  Pallas kernels: 155 us -> 147 us
  local copies, waits for them, and re-layouts: 10.1 us -> 3.2 us
    pallas_call x1, Pallas kernels: 155 us -> 147 us  [body(): pl.pallas_call(kernel, out_shape=jax.ShapeDtypeStruct((TOK, OWN), BF16),...]
    unnamed x23 -> x1, local copies, waits for them, and re-layouts: 5.73 us -> 1.94 us
    slice x6 -> x0, local copies, waits for them, and re-layouts: 1.91 us -> none  [the longest x1 1.1 us: body(): wd[:, :MAIN]]
    concatenate x2 -> x0, local copies, waits for them, and re-layouts: 1.85 us -> none  [the longest x1 1.77 us: body(): jnp.concatenate([w_gate, w_value[:, MAIN:], wd[:, MAIN:], jnp.zeros((HW,...]
where the time goes in v2:
time: 151 us
  Pallas kernels  147 us (97%)
  local copies, waits for them, and re-layouts  3.2 us (2%)
    pallas_call x1, Pallas kernels, body(): pl.pallas_call(kernel, out_shape=jax.ShapeDtypeStruct((TOK, OWN), BF16),...  147 us

profile of v2, /device:TPU:0, one launch (start us, length us, event | category | flops | bytes accessed | tf_op | source)
XLA Modules:
  0.0 150.7 jit_solution(5194290567684060462)
XLA Ops:
  0.0 1.3 broadcast_in_dim.9.seg_ref
  1.3 147.4 %shard_map.145 = bf16[768,384]{1,0:T(8,128)(2,1)} custom-call(bf16[192,1056]{1,0:T(8,128)(2,1)} %wg_ref.1, bf16[192,1056]{1,0:T(8,128)(2,1)} %wv_ref.1, bf16[192,1056]{1,0:T(8,128)(2,1)} %bitcast.7, bf16[192,768]{1,0:T(8,128)(2,1)} %bitcast.8, bf16[192,768]{1,0:T(8,128)(2,1)} %bitcast.9, bf16[192,768]{1,0:T(8,128)(2,1)} %bitcast.10, ...), custom_call_target="tpu_custom_call" | custom-call | tf_op jit(solution)/shard_map/pallas_call | solution.py:656
  148.7 1.9 %copy.17 = bf16[768,384]{1,0:T(8,128)(2,1)} copy(bf16[768,384]{1,0:T(8,128)(2,1)} %shard_map.145) | data formatting | bytes 1179648

commit v3 on v2

v3 whole, which is shorter than its diff:
```python
import jax
import jax.numpy as jnp
from jax import lax
from jax.experimental import pallas as pl
from jax.experimental.pallas import tpu as pltpu
from jax.sharding import Mesh
from jax.sharding import PartitionSpec as P

MESH = pl.DeviceIdType.MESH
F32 = jnp.float32
BF16 = jnp.bfloat16
ABSENT = -1e30
DH = 96
TOK = 768
OWN = 384
HW = 192
MAIN = 1024
GW = 1152
LANES = 2176
PART = 64
EPS = 1e-6
VLIM = 60
SEMS = 104
scope = jax.named_scope


def mod4(v):
    return lax.rem(v + 8, 4)


def dot(a, b, **kw):
    return lax.dot_general(a, b, (((1,), (0,)), ((), ())), preferred_element_type=F32, **kw)


def dot_t(a, b, **kw):
    return lax.dot_general(a, b, (((1,), (1,)), ((), ())), preferred_element_type=F32, **kw)


def dot_c(a, b, **kw):
    return lax.dot_general(a, b, (((0,), (0,)), ((), ())), preferred_element_type=F32, **kw)


def kernel(
    wg_ref,
    wv_ref,
    wd_ref,
    q_hbm,
    k_hbm,
    v_hbm,
    og_hbm,
    wo_ref,
    resid_hbm,
    ig_hbm,
    fg_hbm,
    seg_hbm,
    hg_hbm,
    gain_hbm,
    taps_hbm,
    out_ref,
    W,
    ig_ref,
    fg_ref,
    seg_ref,
    hg_ref,
    gain_ref,
    taps_ref,
    WD0,
    WD1,
    WD2,
    TL,
    X,
    MIX,
    WO,
    WOT,
    QT,
    KT,
    VT,
    OG,
    RB,
    OI,
    NF,
    ST,
    SR,
    MT,
    MR,
    SS,
    RES,
    ACC,
    GT,
    EDGE,
    HD,
    SP,
    RP,
    ZS,
    RL,
    RV,
    sems,
    lsem,
):
    z, x = lax.axis_index("z"), lax.axis_index("x")
    y, c = lax.axis_index("y"), lax.axis_index("c")
    sp = z * 4 + x
    tp = y * 2 + c
    o = 1 - c
    table = {}
    rkey_any = "w"

    def slot(key):
        return table.setdefault(key, len(table))

    def copy(rkey, skey, src, dst, dev):
        return pltpu.make_async_remote_copy(
            src_ref=src,
            dst_ref=dst,
            send_sem=sems.at[slot(("S", skey))],
            recv_sem=sems.at[slot(("R", rkey))],
            device_id=dev,
            device_id_type=MESH,
        )

    def send(rkey, skey, src, dst, dev):
        copy(rkey, skey, src, dst, dev).start()

    partner = (z, x, y, o)

    def recv(rkey, span):
        copy(rkey, rkey_any, span, span, partner).wait_recv()

    def sent(skey, span):
        copy(rkey_any, skey, span, span, partner).wait_send()

    def at_sp(n):
        s = lax.rem(sp + n + 16, 16)
        return (s // 4, lax.rem(s, 4), y, c)

    def at_x(d):
        return (z, mod4(x + d), y, c)

    def at_z(d):
        return (mod4(z + d), x, y, c)

    def at_y(d):
        return (z, x, mod4(y + d), c)

    def at_tp(n):
        t = lax.rem(tp + n, 8)
        return (z, x, t // 2, lax.rem(t, 2))

    peers = [at_x(1), at_x(-1), at_z(1), at_z(-1)]
    peers += [at_tp(n) for n in range(1, 8)]
    peers += [at_sp(n) for n in (1, 2, 3, -1, -2, -3)]
    barrier = pltpu.get_barrier_semaphore()
    for dev in peers:
        pl.semaphore_signal(barrier, inc=1, device_id=dev, device_id_type=MESH)

    local = []

    def bring(src, dst):
        d = pltpu.make_async_copy(src, dst, lsem.at[len(local)])
        d.start()
        local.append(d)

    own_w = pl.ds(pl.multiple_of(sp * HW, 16), HW)
    bring(wg_ref.at[:, 0:MAIN], W.at[own_w, 0:MAIN])
    bring(wv_ref.at[:, 0:MAIN], W.at[own_w, GW:LANES])
    for n, ref in enumerate((wg_ref, wv_ref, wd_ref)):
        bring(ref.at[:, MAIN : MAIN + 32], TL.at[n])
    bring(fg_hbm, fg_ref)
    bring(ig_hbm, ig_ref)
    bring(seg_hbm, seg_ref)
    bring(k_hbm, KT)
    bring(v_hbm, VT)
    bring(q_hbm, QT)
    bring(og_hbm, OG)
    for n, ref in enumerate((WD0, WD1, WD2)):
        bring(
            wd_ref.at[n * PART : (n + 1) * PART, 0:MAIN],
            ref.at[pl.ds(pl.multiple_of(sp * PART, 16), PART), :],
        )
    bring(hg_hbm, hg_ref)
    bring(gain_hbm, gain_ref)
    bring(taps_hbm, taps_ref)
    bring(resid_hbm, RB)
    bring(
        wo_ref.at[:, pl.ds(pl.multiple_of(tp * OWN, 128), OWN)],
        WO.at[pl.ds(pl.multiple_of(tp * HW, 16), HW), :],
    )

    def stage(name, ref, stride, rows, lanes, by_lanes, first):
        x_first = first == "x"
        prim = at_x if x_first else at_z
        secd = at_z if x_first else at_x
        steps = (0, -1, 1, 2)

        def place(dp, ds, half=None):
            zz, xx = (mod4(z + ds), mod4(x + dp)) if x_first else (mod4(z + dp), mod4(x + ds))
            (r0, nr), (l0, nl) = rows, lanes
            if half is not None and by_lanes:
                l0, nl = l0 + half * nl // 2, nl // 2
            elif half is not None:
                r0, nr = r0 + half * nr // 2, nr // 2
            row = pl.multiple_of((zz * 4 + xx) * stride + r0, 16)
            return ref.at[pl.ds(row, nr), pl.ds(l0, nl)]

        def span(k):
            return ref.at[pl.ds(0, k * rows[1]), pl.ds(lanes[0], lanes[1])]

        def primary():
            for d in (1, -1):
                send((name, "p"), name, place(0, 0), place(0, 0), prim(d))

        def second(m):
            p = place(steps[m], 0)
            for d in (1, -1):
                send((name, "s", m), name, p, p, secd(d))

        def relay():
            recv((name, "p"), span(2))
            for d in (1, -1):
                p = place(-d, 0, 0 if d == 1 else 1)
                send((name, "pf"), name, p, p, prim(d))

        def across(m):
            recv((name, "s", m), span(2))
            for d in (1, -1):
                p = place(steps[m], -d, 0 if d == 1 else 1)
                send((name, "sf"), name, p, p, secd(d))

        def far():
            recv((name, "pf"), span(1))
            second(3)

        def done():
            recv((name, "sf"), span(4))

        def out():
            sent(name, span(15))

        return primary, second, relay, across, far, done, out

    def run(stages, what, *args):
        k = ("primary", "second", "relay", "across", "far", "done", "out").index(what)
        for st in stages:
            st[k](*args)

    gv = (
        stage("g", W, HW, (0, HW), (0, GW), False, "x"),
        stage("v", W, HW, (0, HW), (GW, MAIN), False, "z"),
    )

    def down_stage(n, ref, cut):
        return (
            stage(("da", n), ref, PART, (0, cut), (0, MAIN), True, "x"),
            stage(("db", n), ref, PART, (cut, PART - cut), (0, MAIN), True, "z"),
        )

    d0, d1, d2 = down_stage(0, WD0, 16), down_stage(1, WD1, 32), down_stage(2, WD2, 32)

    def over_tp(name, blk, span):
        def g0():
            b = blk(y, c)
            for d in (1, -1):
                send((name, "y"), name, b, b, at_y(d))
            send((name, "o"), name, b, b, partner)

        def g1():
            recv((name, "y"), span(2))
            for d in (1, -1):
                h = blk(mod4(y - d), c, 0 if d == 1 else 1)
                send((name, "f"), name, h, h, at_y(d))
            for d in (1, -1):
                b = blk(mod4(y - d), c)
                send((name, "o"), name, b, b, partner)

        def g2():
            recv((name, "f"), span(1))
            b = blk(mod4(y + 2), c)
            send((name, "o"), name, b, b, partner)

        def g3():
            recv((name, "o"), span(4))

        def out():
            sent(name, span(7))

        return g0, g1, g2, g3, out

    def mix_block(yy, cc, half=None):
        r0, nr = (0, HW) if half is None else (half * DH, DH)
        return MIX.at[pl.ds(pl.multiple_of((yy * 2 + cc) * HW + r0, 16), nr), :]

    def x_block(yy, cc, half=None):
        rows = slice(None) if half is None else pl.ds(half * OWN, OWN)
        return X.at[rows, pl.ds(pl.multiple_of((yy * 2 + cc) * OWN, 128), OWN)]

    mix_g = over_tp("m", mix_block, lambda k: MIX.at[pl.ds(0, k * HW), :])
    x_g = over_tp("x", x_block, lambda k: X.at[:, pl.ds(0, k * OWN)])

    for d in local[:5]:
        d.wait()
    tails = jnp.concatenate([TL[0], TL[1], TL[2], jnp.zeros((HW, 32), BF16)], axis=1)
    W[own_w, MAIN:GW] = tails
    with scope("barrier"):
        pl.semaphore_wait(barrier, len(peers))
    run(gv[1:], "primary")
    run(gv[:1], "primary")
    for n in range(1, 8):
        t = lax.rem(tp + n, 8)
        src = wo_ref.at[:, pl.ds(pl.multiple_of(t * OWN, 128), OWN)]
        dst = WO.at[pl.ds(pl.multiple_of(tp * HW, 16), HW), :]
        send("w", "w", src, dst, at_tp(n))

    lane = lax.broadcasted_iota(jnp.int32, (8, TOK), 1)
    row8 = lax.broadcasted_iota(jnp.int32, (8, TOK), 0)
    for d in local[5:8]:
        d.wait()
    seg = seg_ref[...].reshape(1, TOK).astype(F32)
    fg = jnp.where(row8 == 0, fg_ref[0:1], fg_ref[1:2])
    e = jnp.exp(-jnp.abs(fg))
    log1p = jnp.where(e < 1e-2, e * (1.0 - e * (0.5 - e * (1.0 / 3.0))), jnp.log(1.0 + e))
    cum = jnp.minimum(fg, 0.0) - log1p
    shift = 1
    while shift < TOK:
        cum = cum + jnp.where(lane >= shift, pltpu.roll(cum, shift, 1), 0.0)
        shift *= 2
    b = [ig_ref[h : h + 1] - cum[h : h + 1] for h in range(2)]
    end = [cum[h : h + 1, TOK - 1 :] for h in range(2)]
    first, last, second_last = seg[:, :1], seg[:, TOK - 1 :], seg[:, TOK - 2 : TOK - 1]
    for d in local[8:12]:
        d.wait()
    ST[...] = jnp.zeros_like(ST)
    peak = []
    for h in range(2):
        hs = slice(h * DH, h * DH + DH)
        top = jnp.max(jnp.where(seg == last, b[h], ABSENT), axis=1, keepdims=True)
        peak.append(top)
        w = jnp.where(seg == last, jnp.exp(jnp.minimum(b[h] - top, 0.0)), 0.0) * DH**-0.5
        ST[hs, 0:DH] = dot_t(VT[hs, :], (KT[hs, :].astype(F32) * w).astype(BF16)).astype(BF16)
    meta_row = lax.broadcasted_iota(jnp.int32, (8, 128), 0)
    meta = jnp.zeros((8, 128), F32)
    for n, value in enumerate((end[0] + peak[0], end[1] + peak[1], end[0], end[1], first, last, second_last)):
        meta = jnp.where(meta_row == n, value, meta)
    MT[...] = meta
    for n in range(1, 5):
        send("st", "st", ST, SR.at[n - 1], at_sp(n))
        send("mt", "mt", MT, MR.at[n - 1], at_sp(n))
    run(gv, "second", 0)

    rows = jnp.where(row8 == 0, b[0], jnp.where(row8 == 1, b[1], seg))
    cols = jnp.transpose(jnp.concatenate([rows, jnp.zeros((120, TOK), F32)], axis=0))
    seg_c = cols[:, 2:3]
    tops = [[], []]
    for i in range(3):
        t0, ns = i * 256, (i + 1) * 256
        ts = slice(t0, t0 + 256)
        s_at = lax.broadcasted_iota(jnp.int32, (ns, 256), 0)
        t_at = lax.broadcasted_iota(jnp.int32, (ns, 256), 1) + t0
        mask = (seg_c[:ns] == seg[:, ts]) & (s_at <= t_at)
        for h in range(2):
            hs = slice(h * DH, h * DH + DH)
            masked = jnp.where(mask, cols[:ns, h : h + 1], ABSENT)
            top = jnp.max(masked, axis=0, keepdims=True)
            scores = dot_c(KT[hs, 0:ns], QT[hs, ts]) * (jnp.exp(masked - top) * DH**-0.5)
            OI[hs, ts] = dot(VT[hs, 0:ns], scores.astype(BF16))
            tops[h].append(top)

    with scope("relay"):
        run(gv, "relay")
        run(gv, "second", 1)
        run(gv, "second", 2)

    dec = [jnp.zeros((1, 128), F32)] * 2
    cand = [[], []]
    first_l = jnp.broadcast_to(first, (1, 128))
    with scope("state"):
        recv("st", SR)
        recv("mt", MR)
    for n in range(1, 5):
        m = MR[n - 1]
        valid = (m[5:6] == first_l) & (sp >= n)
        for h in range(2):
            cand[h].append(jnp.where(valid, m[h : h + 1] + dec[h], ABSENT))
            dec[h] = dec[h] + m[2 + h : 3 + h]
    for d in local[12:18]:
        d.wait()
    gain_at = lax.broadcasted_iota(jnp.int32, (HW, HW), 0) == lax.broadcasted_iota(jnp.int32, (HW, HW), 1)
    gain_c = jnp.sum(jnp.where(gain_at, hg_ref[...], 0.0), axis=1, keepdims=True)
    for h in range(2):
        hs = slice(h * DH, h * DH + DH)
        pin = jnp.maximum(
            jnp.maximum(cand[h][0], cand[h][1]), jnp.maximum(cand[h][2], cand[h][3])
        )
        state = jnp.zeros((DH, 128), F32)
        for n in range(4):
            state = state + jnp.exp(cand[h][n] - pin) * SR[n, hs, :].astype(F32)
        inter = dot(state[:, 0:DH].astype(BF16), QT[hs, :])
        m_in = jnp.concatenate(tops[h], axis=1)
        m_pin = jnp.where(seg == first, pin[:, :1], ABSENT)
        m_all = jnp.maximum(m_in, m_pin)
        memory = jnp.exp(m_in - m_all) * OI[hs, :] + jnp.exp(m_pin - m_all) * inter
        mean = jnp.sum(memory * memory, axis=0, keepdims=True) * (1.0 / DH)
        mix = memory * lax.rsqrt(mean + 1.0) * gain_c[hs] * jax.nn.sigmoid(OG[hs, :].astype(F32))
        MIX[pl.ds(pl.multiple_of(tp * HW + h * DH, 16), DH), :] = mix.astype(BF16)
    with scope("mix0"):
        mix_g[0]()
    with scope("across0"):
        run(gv, "across", 0)

    before = MR[0]
    there = sp >= 1
    last_before = jnp.where(there, before[5:6, :1], -1.0)
    second_before = jnp.where(there, before[6:7, :1], -1.0)
    seg8 = jnp.broadcast_to(seg, (8, TOK))
    one_back = jnp.where(lane == 0, last_before, pltpu.roll(seg8, 1, 1))
    two_back = jnp.where(
        lane == 0, second_before, jnp.where(lane == 1, last_before, pltpu.roll(seg8, 2, 1))
    )
    flags = jnp.where(
        row8 == 0, jnp.where(one_back == seg, 1.0, 0.0), jnp.where(two_back == seg, 1.0, 0.0)
    )
    NF[...] = jnp.transpose(jnp.concatenate([flags, jnp.zeros((120, TOK), F32)], axis=0))
    with scope("wo"):
        for d in local[18:]:
            d.wait()
        recv("w", WO.at[pl.ds(0, 7 * HW), :])
        WOT[...] = jnp.transpose(WO[...])

    with scope("mix1"):
        mix_g[1]()
    with scope("far"):
        run(gv, "far")
    with scope("mix2"):
        mix_g[2]()
    with scope("mix3"):
        mix_g[3]()

    gain = gain_ref[:, pl.ds(pl.multiple_of(tp * OWN, 128), OWN)]
    res = RB[...].astype(F32) + jnp.transpose(dot(WOT[...], MIX[...]))
    RES[...] = res
    X[:, pl.ds(pl.multiple_of(tp * OWN, 128), OWN)] = (res * gain).astype(BF16)
    x_g[0]()
    SS[tp] = dot_t(jnp.ones((8, OWN), F32), res * res, precision=lax.Precision.HIGHEST)
    for n in range(1, 8):
        send("q", "q", SS.at[tp], SS.at[tp], at_tp(n))
    with scope("across1"):
        run(gv, "across", 1)
    with scope("across2"):
        run(gv, "across", 2)
    with scope("x1"):
        x_g[1]()
    with scope("x2"):
        x_g[2]()
    with scope("x3"):
        x_g[3]()
    run(d0, "primary")
    run(d0, "second", 0)
    with scope("across3"):
        run(gv, "across", 3)
    with scope("sq"):
        recv("q", SS.at[pl.ds(0, 7)])
        total = SS[0]
        for n in range(1, 8):
            total = total + SS[n]
    scale_row = lax.rsqrt(total * (1.0 / 3072.0) + EPS)
    NF[:, 2:3] = jnp.transpose(jnp.concatenate([scale_row, jnp.zeros((120, TOK), F32)], axis=0))[:, 0:1]

    def tile256(n, at):
        return pl.ds(pl.multiple_of(n * 256 + at, 128), 256)

    def by_row(lanes, steps):
        acc = None
        for d in steps:
            k = pl.ds(pl.multiple_of(mod4(z + d) * 768, 128), 768)
            part = dot(X[:, k], W[k, lanes])
            acc = part if acc is None else acc + part
        return acc

    def by_pair(lanes, which):
        acc = None
        for zz in range(4):
            k = pl.ds(pl.multiple_of(zz * 768 + which * OWN, 128), OWN)
            part = dot(X[:, k], W[k, lanes])
            acc = part if acc is None else acc + part
        return acc

    here = x // 2
    with scope("partial"):

        def early(n, _):
            ACC[:, tile256(n, 0)] = by_row(tile256(n, 0), (0, 1, -1))
            ACC[:, tile256(n, GW)] = by_pair(tile256(n, GW), here)
            return 0

        lax.fori_loop(0, 4, early, 0)
        ACC[:, MAIN:GW] = by_row(slice(MAIN, GW), (0, 1, -1))

    with scope("d0relay"):
        run(d0, "relay")
        run(d0, "second", 1)
        run(d0, "second", 2)
    with scope("done"):
        run(gv, "done")
    with scope("p1"):
        run(d0, "across", 0)
        run(d0, "far")
        run(d1, "primary")
        run(d1, "second", 0)
    scale = NF[:, 2:3]
    with scope("gate"):

        def gate_tile(n, _):
            l = tile256(n, 0)
            GT[:, l] = ((ACC[:, l] + by_row(l, (2,))) * scale).astype(BF16)
            return 0

        lax.fori_loop(0, 4, gate_tile, 0)
        l = slice(MAIN, GW)
        GT[:, l] = ((ACC[:, l] + by_row(l, (2,))) * scale).astype(BF16)
    send("e", "e", GT.at[TOK - 16 : TOK, :], EDGE, at_sp(1))
    with scope("p2"):
        run(d0, "across", 1)
        run(d1, "relay")
        run(d1, "second", 1)
        run(d1, "second", 2)

    def hidden_of(lanes, width, taps, value):
        g = GT[:, lanes].astype(F32)
        edge = EDGE[:, lanes].astype(F32)
        t_at = lax.broadcasted_iota(jnp.int32, (TOK, width), 0)
        near = NF[:, 0:1] > 0.5
        far = NF[:, 1:2] > 0.5
        g1 = jnp.where(t_at == 0, edge[15:16], pltpu.roll(g, 1, 0))
        g2 = jnp.where(
            t_at == 0, edge[14:15], jnp.where(t_at == 1, edge[15:16], pltpu.roll(g, 2, 0))
        )
        conv = taps[2:3] * g + taps[1:2] * jnp.where(near, g1, 0.0) + taps[0:1] * jnp.where(far, g2, 0.0)
        return conv / (1.0 + jnp.exp(-conv)) * value

    def value_sum(n, _):
        l = tile256(n, GW)
        ACC[:, l] = ACC[:, l] + by_pair(l, 1 - here)
        return 0

    with scope("value"):
        lax.fori_loop(0, 2, value_sum, 0)
    with scope("p3"):
        run(d0, "across", 2)
        run(d1, "across", 0)
    with scope("value"):
        lax.fori_loop(2, 4, value_sum, 0)
    with scope("p4"):
        run(d0, "across", 3)
        run(d1, "far")
        run(d2, "primary")
        run(d2, "second", 0)
    with scope("edge"):
        recv("e", EDGE)

    with scope("hidden"):

        def hidden_tile(n, _):
            value = (ACC[:, tile256(n, GW)] * scale).astype(BF16).astype(F32)
            l = tile256(n, 0)
            HD[:, l] = hidden_of(l, 256, taps_ref[:, l], value).astype(BF16)
            return 0

        lax.fori_loop(0, 4, hidden_tile, 0)
        tail = slice(MAIN, GW)
        taps_tail = jnp.concatenate([taps_ref[:, MAIN : MAIN + 32], jnp.zeros((3, 96), F32)], axis=1)
        value_tail = pltpu.roll(GT[:, tail].astype(F32), 96, 1)
        HD[:, tail] = pltpu.roll(hidden_of(tail, 128, taps_tail, value_tail), 64, 1).astype(BF16)
    with scope("p5"):
        run(d1, "across", 1)
        run(d2, "relay")
        run(d2, "second", 1)
        run(d2, "second", 2)
        run(d0, "done")

    downs = (WD0, WD1, WD2)

    def partials(p, da, db, cc):
        mains, ends = [], []
        for d in (da, db):
            j = mod4(y + d) * 2 + cc
            mains.append(downs[p][pl.ds(pl.multiple_of(j * 128, 128), 128), :])
            for k in range(2):
                at = pl.multiple_of((j * 2 + k) * HW + p * PART, 16)
                ends.append(W[pl.ds(at, PART), MAIN:GW])
        return dot_t(HD[:, 0:MAIN], jnp.concatenate(mains, axis=0)) + dot_t(
            HD[:, MAIN:GW], jnp.concatenate(ends, axis=0)
        )

    order = (2, 1, -1, 0)

    def at_po(p, m):
        return pl.ds(m * OWN + p * 128, 128)

    def give(p, n):
        both = partials(p, order[n], order[n + 1], o).astype(BF16)
        for k in range(2):
            SP[n + k, :, pl.ds(p * 128, 128)] = both[:, k * 128 : (k + 1) * 128]
            l = pl.ds(p * 128, 128)
            send(("sp", p, n), "sp", SP.at[n + k, :, l], RP.at[n + k, :, l], partner)

    def keep(p, n):
        l = pl.ds(p * 128, 128)
        mine = partials(p, order[n], order[n + 1], c)
        with scope("sp%d" % n):
            recv(("sp", p, n), RP.at[pl.ds(n, 2), :, l])
        for k in range(2):
            m, d = n + k, order[n + k]
            both = mine[:, k * 128 : (k + 1) * 128] + RP[m, :, l].astype(F32)
            if d == 2:
                ZS[0, :, l] = both.astype(BF16)
                send(("rl", p), "rl", ZS.at[0, pl.ds(0, OWN), l], RL.at[0, :, l], at_y(1))
                send(("rl", p), "rl", ZS.at[0, pl.ds(OWN, OWN), l], RL.at[1, :, l], at_y(-1))
            else:
                ACC[:, at_po(p, m)] = both
                if d != 0:
                    r = pl.ds(OWN if d == 1 else 0, OWN)
                    ZS[m, r, l] = both[OWN:, :].astype(BF16) if d == 1 else both[:OWN, :].astype(BF16)
                    send(("rv", p), "rv", ZS.at[m, r, l], RV.at[m - 1, r, l], at_y(d))

    def pass_on(p):
        l = pl.ds(p * 128, 128)
        with scope("rl"):
            recv(("rl", p), RL.at[:, :, l])
        for n, d in ((1, 1), (2, -1)):
            r = pl.ds(0 if d == 1 else OWN, OWN)
            ZS[n, r, l] = (ACC[r, at_po(p, n)] + RL[n - 1, :, l].astype(F32)).astype(BF16)
            send(("rv", p), "rv", ZS.at[n, r, l], RV.at[n - 1, r, l], at_y(d))

    def collect(p):
        l = pl.ds(p * 128, 128)
        with scope("rv%d" % p):
            recv(("rv", p), RV.at[:, :, l])
        return ACC[:, at_po(p, 3)] + RV[0, :, l].astype(F32) + RV[1, :, l].astype(F32)

    with scope("reduce0"):
        give(0, 0)
        run(d1, "across", 2)
        give(0, 2)
        run(d2, "across", 0)
        keep(0, 0)
        run(d1, "across", 3)
        keep(0, 2)
        run(d2, "far")
    with scope("p6"):
        run(d2, "across", 1)
        run(d1, "done")
        pass_on(0)
    with scope("reduce1"):
        give(1, 0)
        run(d2, "across", 2)
        give(1, 2)
        run(d2, "across", 3)
        keep(1, 0)
        keep(1, 2)
    with scope("p7"):
        pass_on(1)
        run(d2, "done")
    with scope("reduce2"):
        give(2, 0)
        give(2, 2)
        keep(2, 0)
        keep(2, 2)
        pass_on(2)
    with scope("final"):
        low = lax.broadcasted_iota(jnp.int32, (TOK, 128), 1) < 64
        part0 = collect(0)
        turned = pltpu.roll(collect(1), 64, 1)
        out_ref[:, 0:128] = (RES[:, 0:128] + jnp.where(low, part0, turned)).astype(BF16)
        part2 = collect(2)
        out_ref[:, 128:256] = (RES[:, 128:256] + jnp.where(low, part2, part0)).astype(BF16)
        out_ref[:, 256:384] = (RES[:, 256:384] + jnp.where(low, turned, part2)).astype(BF16)
    with scope("sent"):
        for part in (gv, d0, d1, d2):
            run(part, "out")
        mix_g[4]()
        x_g[4]()
        sent("w", WO.at[pl.ds(0, 7 * HW), :])
        sent("st", SR)
        sent("mt", MR)
        sent("q", SS.at[pl.ds(0, 7)])
        sent("e", EDGE)
        sent("sp", SP)
        sent("rl", RL)
        sent("rv", RV)


def body(
    resid,
    query,
    keys,
    values,
    out_gate,
    in_gate,
    forget,
    doc_ids,
    head_gain,
    w_out,
    ffn_gain,
    w_gate,
    w_value,
    conv_taps,
    w_down,
):
    vmem = pl.BlockSpec(memory_space=pltpu.VMEM)
    hbm = pl.BlockSpec(memory_space=pl.ANY)
    return pl.pallas_call(
        kernel,
        out_shape=jax.ShapeDtypeStruct((TOK, OWN), BF16),
        in_specs=[hbm] * 15,
        out_specs=vmem,
        scratch_shapes=[
            pltpu.VMEM((3072, LANES), BF16),
            pltpu.VMEM((2, TOK), F32),
            pltpu.VMEM((2, TOK), F32),
            pltpu.VMEM((TOK,), jnp.int32),
            pltpu.VMEM((1, HW), F32),
            pltpu.VMEM((1, 3072), F32),
            pltpu.VMEM((3, 1056), F32),
            pltpu.VMEM((16 * PART, MAIN), BF16),
            pltpu.VMEM((16 * PART, MAIN), BF16),
            pltpu.VMEM((16 * PART, MAIN), BF16),
            pltpu.VMEM((3, HW, 32), BF16),
            pltpu.VMEM((TOK, 3072), BF16),
            pltpu.VMEM((1536, TOK), BF16),
            pltpu.VMEM((1536, OWN), BF16),
            pltpu.VMEM((OWN, 1536), BF16),
            pltpu.VMEM((HW, TOK), BF16),
            pltpu.VMEM((HW, TOK), BF16),
            pltpu.VMEM((HW, TOK), BF16),
            pltpu.VMEM((HW, TOK), BF16),
            pltpu.VMEM((TOK, OWN), BF16),
            pltpu.VMEM((HW, TOK), F32),
            pltpu.VMEM((TOK, 128), F32),
            pltpu.VMEM((HW, 128), BF16),
            pltpu.VMEM((4, HW, 128), BF16),
            pltpu.VMEM((8, 128), F32),
            pltpu.VMEM((4, 8, 128), F32),
            pltpu.VMEM((8, 8, TOK), F32),
            pltpu.VMEM((TOK, OWN), F32),
            pltpu.VMEM((TOK, LANES), F32),
            pltpu.VMEM((TOK, GW), BF16),
            pltpu.VMEM((16, GW), BF16),
            pltpu.VMEM((TOK, GW), BF16),
            pltpu.VMEM((4, TOK, OWN), BF16),
            pltpu.VMEM((4, TOK, OWN), BF16),
            pltpu.VMEM((3, TOK, OWN), BF16),
            pltpu.VMEM((2, OWN, OWN), BF16),
            pltpu.VMEM((2, TOK, OWN), BF16),
            pltpu.SemaphoreType.DMA((SEMS,)),
            pltpu.SemaphoreType.DMA((20,)),
        ],
        compiler_params=pltpu.CompilerParams(
            collective_id=0, has_side_effects=True, vmem_limit_bytes=VLIM * 1024 * 1024
        ),
    )(
        w_gate,
        w_value,
        w_down.T,
        query.T,
        keys.T,
        values.T,
        out_gate.T,
        w_out,
        resid,
        in_gate,
        forget,
        doc_ids,
        head_gain[None],
        ffn_gain[None],
        conv_taps,
    )


def solution(mesh):
    torus = Mesh(mesh.devices.reshape(4, 4, 4, 2), ("z", "x", "y", "c"))
    sp, tp = ("z", "x"), ("y", "c")
    placed = (
        P(sp, tp),
        P(sp, tp),
        P(sp, tp),
        P(sp, tp),
        P(sp, tp),
        P(tp, sp),
        P(tp, sp),
        P(sp),
        P(tp),
        P(tp, None),
        P(),
        P(sp, tp),
        P(sp, tp),
        P(None, tp),
        P(tp, sp),
    )
    return jax.shard_map(body, mesh=torus, in_specs=placed, out_specs=P(sp, tp), check_vma=False)
```

time: 151 us -> 140 us (0.927)
  Pallas kernels: 147 us -> 138 us
    pallas_call x1, Pallas kernels: 147 us -> 138 us  [body(): pl.pallas_call(kernel, out_shape=jax.ShapeDtypeStruct((TOK, OWN), BF16),...]
where the time goes in v3:
time: 140 us
  Pallas kernels  138 us (99%)
  local copies, waits for them, and re-layouts  1.94 us (1%)
    pallas_call x1, Pallas kernels, body(): pl.pallas_call(kernel, out_shape=jax.ShapeDtypeStruct((TOK, OWN), BF16),...  138 us

profile of v3, /device:TPU:0, one launch (start us, length us, event | category | flops | bytes accessed | tf_op | source)
XLA Modules:
  0.0 140.1 jit_solution(13604953755202318555)
XLA Ops:
  0.0 138.2 %shard_map.145 = bf16[768,384]{1,0:T(8,128)(2,1)} custom-call(bf16[192,1056]{1,0:T(8,128)(2,1)} %wg_ref.1, bf16[192,1056]{1,0:T(8,128)(2,1)} %wv_ref.1, bf16[192,1056]{1,0:T(8,128)(2,1)} %bitcast.7, bf16[192,768]{1,0:T(8,128)(2,1)} %bitcast.8, bf16[192,768]{1,0:T(8,128)(2,1)} %bitcast.9, bf16[192,768]{1,0:T(8,128)(2,1)} %bitcast.10, ...), custom_call_target="tpu_custom_call" | custom-call | tf_op jit(solution)/shard_map/pallas_call | solution.py:710
  138.2 1.9 %copy.17 = bf16[768,384]{1,0:T(8,128)(2,1)} copy(bf16[768,384]{1,0:T(8,128)(2,1)} %shard_map.145) | data formatting | bytes 1179648

commit v4 on v3

--- a/solution.py
+++ b/solution.py
@@ -20,7 +20,7 @@
 PART = 64
 EPS = 1e-6
 VLIM = 60
-SEMS = 104
+SEMS = 94
 scope = jax.named_scope
 
 
@@ -498,13 +498,13 @@
         run(d0, "relay")
         run(d0, "second", 1)
         run(d0, "second", 2)
+        run(d1, "primary")
+        run(d1, "second", 0)
     with scope("done"):
         run(gv, "done")
     with scope("p1"):
         run(d0, "across", 0)
         run(d0, "far")
-        run(d1, "primary")
-        run(d1, "second", 0)
     scale = NF[:, 2:3]
     with scope("gate"):
 
@@ -519,9 +519,7 @@
     send("e", "e", GT.at[TOK - 16 : TOK, :], EDGE, at_sp(1))
     with scope("p2"):
         run(d0, "across", 1)
-        run(d1, "relay")
-        run(d1, "second", 1)
-        run(d1, "second", 2)
+        run(d0, "across", 2)
 
     def hidden_of(lanes, width, taps, value):
         g = GT[:, lanes].astype(F32)
@@ -544,15 +542,16 @@
     with scope("value"):
         lax.fori_loop(0, 2, value_sum, 0)
     with scope("p3"):
-        run(d0, "across", 2)
-        run(d1, "across", 0)
+        run(d1, "relay")
     with scope("value"):
         lax.fori_loop(2, 4, value_sum, 0)
     with scope("p4"):
         run(d0, "across", 3)
-        run(d1, "far")
+        run(d1, "second", 1)
+        run(d1, "second", 2)
         run(d2, "primary")
         run(d2, "second", 0)
+        run(d1, "across", 0)
     with scope("edge"):
         recv("e", EDGE)
 
@@ -570,17 +569,14 @@
         value_tail = pltpu.roll(GT[:, tail].astype(F32), 96, 1)
         HD[:, tail] = pltpu.roll(hidden_of(tail, 128, taps_tail, value_tail), 64, 1).astype(BF16)
     with scope("p5"):
-        run(d1, "across", 1)
-        run(d2, "relay")
-        run(d2, "second", 1)
-        run(d2, "second", 2)
+        run(d1, "far")
         run(d0, "done")
 
     downs = (WD0, WD1, WD2)
 
-    def partials(p, da, db, cc):
+    def partials(p, cc):
         mains, ends = [], []
-        for d in (da, db):
+        for d in order:
             j = mod4(y + d) * 2 + cc
             mains.append(downs[p][pl.ds(pl.multiple_of(j * 128, 128), 128), :])
             for k in range(2):
@@ -595,31 +591,30 @@
     def at_po(p, m):
         return pl.ds(m * OWN + p * 128, 128)
 
-    def give(p, n):
-        both = partials(p, order[n], order[n + 1], o).astype(BF16)
-        for k in range(2):
-            SP[n + k, :, pl.ds(p * 128, 128)] = both[:, k * 128 : (k + 1) * 128]
-            l = pl.ds(p * 128, 128)
-            send(("sp", p, n), "sp", SP.at[n + k, :, l], RP.at[n + k, :, l], partner)
-
-    def keep(p, n):
+    def give(p):
         l = pl.ds(p * 128, 128)
-        mine = partials(p, order[n], order[n + 1], c)
-        with scope("sp%d" % n):
-            recv(("sp", p, n), RP.at[pl.ds(n, 2), :, l])
-        for k in range(2):
-            m, d = n + k, order[n + k]
-            both = mine[:, k * 128 : (k + 1) * 128] + RP[m, :, l].astype(F32)
+        both = partials(p, o).astype(BF16)
+        for n in range(4):
+            SP[n, :, l] = both[:, n * 128 : (n + 1) * 128]
+            send(("sp", p), "sp", SP.at[n, :, l], RP.at[n, :, l], partner)
+
+    def keep(p):
+        l = pl.ds(p * 128, 128)
+        mine = partials(p, c)
+        with scope("sp"):
+            recv(("sp", p), RP.at[:, :, l])
+        for n, d in enumerate(order):
+            both = mine[:, n * 128 : (n + 1) * 128] + RP[n, :, l].astype(F32)
             if d == 2:
                 ZS[0, :, l] = both.astype(BF16)
                 send(("rl", p), "rl", ZS.at[0, pl.ds(0, OWN), l], RL.at[0, :, l], at_y(1))
                 send(("rl", p), "rl", ZS.at[0, pl.ds(OWN, OWN), l], RL.at[1, :, l], at_y(-1))
             else:
-                ACC[:, at_po(p, m)] = both
+                ACC[:, at_po(p, n)] = both
                 if d != 0:
                     r = pl.ds(OWN if d == 1 else 0, OWN)
-                    ZS[m, r, l] = both[OWN:, :].astype(BF16) if d == 1 else both[:OWN, :].astype(BF16)
-                    send(("rv", p), "rv", ZS.at[m, r, l], RV.at[m - 1, r, l], at_y(d))
+                    ZS[n, r, l] = both[OWN:, :].astype(BF16) if d == 1 else both[:OWN, :].astype(BF16)
+                    send(("rv", p), "rv", ZS.at[n, r, l], RV.at[n - 1, r, l], at_y(d))
 
     def pass_on(p):
         l = pl.ds(p * 128, 128)
@@ -636,43 +631,56 @@
             recv(("rv", p), RV.at[:, :, l])
         return ACC[:, at_po(p, 3)] + RV[0, :, l].astype(F32) + RV[1, :, l].astype(F32)
 
-    with scope("reduce0"):
-        give(0, 0)
+    with scope("give0"):
+        give(0)
+    with scope("p6"):
+        run(d1, "across", 1)
+        run(d2, "relay")
+        run(d2, "second", 1)
+        run(d2, "second", 2)
+    with scope("keep0"):
+        keep(0)
+    with scope("p7"):
         run(d1, "across", 2)
-        give(0, 2)
+        run(d1, "across", 3)
         run(d2, "across", 0)
-        keep(0, 0)
-        run(d1, "across", 3)
-        keep(0, 2)
         run(d2, "far")
-    with scope("p6"):
+    with scope("p8"):
         run(d2, "across", 1)
         run(d1, "done")
+    with scope("give1"):
+        give(1)
+    with scope("p8b"):
+        run(d2, "across", 2)
+        run(d2, "across", 3)
+    with scope("pass0"):
         pass_on(0)
-    with scope("reduce1"):
-        give(1, 0)
-        run(d2, "across", 2)
-        give(1, 2)
-        run(d2, "across", 3)
-        keep(1, 0)
-        keep(1, 2)
-    with scope("p7"):
+    with scope("keep1"):
+        keep(1)
+    with scope("p10"):
+        run(d2, "done")
+    with scope("give2"):
+        give(2)
+    with scope("pass1"):
         pass_on(1)
-        run(d2, "done")
-    with scope("reduce2"):
-        give(2, 0)
-        give(2, 2)
-        keep(2, 0)
-        keep(2, 2)
+    with scope("keep2"):
+        keep(2)
+    with scope("pass2"):
         pass_on(2)
-    with scope("final"):
+    with scope("final0"):
         low = lax.broadcasted_iota(jnp.int32, (TOK, 128), 1) < 64
         part0 = collect(0)
         turned = pltpu.roll(collect(1), 64, 1)
         out_ref[:, 0:128] = (RES[:, 0:128] + jnp.where(low, part0, turned)).astype(BF16)
-        part2 = collect(2)
-        out_ref[:, 128:256] = (RES[:, 128:256] + jnp.where(low, part2, part0)).astype(BF16)
-        out_ref[:, 256:384] = (RES[:, 256:384] + jnp.where(low, turned, part2)).astype(BF16)
+        RES[:, 128:256] = RES[:, 128:256] + jnp.where(low, ACC[:, at_po(2, 3)], part0)
+        RES[:, 256:384] = RES[:, 256:384] + jnp.where(low, turned, ACC[:, at_po(2, 3)])
+    with scope("final"):
+        l = pl.ds(256, 128)
+        with scope("rv2"):
+            recv(("rv", 2), RV.at[:, :, l])
+        part2 = RV[0, :, l].astype(F32) + RV[1, :, l].astype(F32)
+        out_ref[:, 128:256] = (RES[:, 128:256] + jnp.where(low, part2, 0.0)).astype(BF16)
+        out_ref[:, 256:384] = (RES[:, 256:384] + jnp.where(low, 0.0, part2)).astype(BF16)
     with scope("sent"):
         for part in (gv, d0, d1, d2):
             run(part, "out")
@@ -686,6 +694,8 @@
         sent("sp", SP)
         sent("rl", RL)
         sent("rv", RV)
+    if len(table) != SEMS:
+        raise ValueError(len(table))
 
 
 def body(
@@ -709,7 +719,7 @@
     hbm = pl.BlockSpec(memory_space=pl.ANY)
     return pl.pallas_call(
         kernel,
-        out_shape=jax.ShapeDtypeStruct((TOK, OWN), BF16),
+        out_shape=pltpu.VMEM((TOK, OWN), BF16),
         in_specs=[hbm] * 15,
         out_specs=vmem,
         scratch_shapes=[

time: 140 us -> 133 us (0.950)
  Pallas kernels: 138 us -> 132 us
    pallas_call x1, Pallas kernels: 138 us -> 132 us  [body(): pl.pallas_call(kernel, out_shape=pltpu.VMEM((TOK, OWN), BF16), in_specs=[...]
where the time goes in v4:
time: 133 us
  Pallas kernels  132 us (99%)
    pallas_call x1, Pallas kernels, body(): pl.pallas_call(kernel, out_shape=pltpu.VMEM((TOK, OWN), BF16), in_specs=[...  132 us

profile of v4, /device:TPU:0, one launch (start us, length us, event | category | flops | bytes accessed | tf_op | source)
XLA Modules:
  0.0 132.5 jit_solution(5218099246630545580)
XLA Ops:
  0.0 131.7 %shard_map.145 = bf16[768,384]{1,0:T(8,128)(2,1)S(1)} custom-call(bf16[192,1056]{1,0:T(8,128)(2,1)} %wg_ref.1, bf16[192,1056]{1,0:T(8,128)(2,1)} %wv_ref.1, bf16[192,1056]{1,0:T(8,128)(2,1)} %bitcast.7, bf16[192,768]{1,0:T(8,128)(2,1)} %bitcast.8, bf16[192,768]{1,0:T(8,128)(2,1)} %bitcast.9, bf16[192,768]{1,0:T(8,128)(2,1)} %bitcast.10, ...), custom_call_target="tpu_custom_call" | custom-call | tf_op jit(solution)/shard_map/pallas_call | solution.py:720
  131.7 0.8 copy.17

commit v5 on v4

--- a/solution.py
+++ b/solution.py
@@ -19,8 +19,9 @@
 LANES = 2176
 PART = 64
 EPS = 1e-6
+EVERY, FAR, REST = (0, 1, 2, 3), (0,), (1, 2, 3)
 VLIM = 60
-SEMS = 94
+SEMS = 95
 scope = jax.named_scope
 
 
@@ -192,13 +193,14 @@
         secd = at_z if x_first else at_x
         steps = (0, -1, 1, 2)
 
-        def place(dp, ds, half=None):
+        def place(dp, ds, half=None, shift=0):
             zz, xx = (mod4(z + ds), mod4(x + dp)) if x_first else (mod4(z + dp), mod4(x + ds))
             (r0, nr), (l0, nl) = rows, lanes
             if half is not None and by_lanes:
                 l0, nl = l0 + half * nl // 2, nl // 2
             elif half is not None:
-                r0, nr = r0 + half * nr // 2, nr // 2
+                upper = nr // 2 - shift
+                r0, nr = (r0 + upper, nr - upper) if half else (r0, upper)
             row = pl.multiple_of((zz * 4 + xx) * stride + r0, 16)
             return ref.at[pl.ds(row, nr), pl.ds(l0, nl)]
 
@@ -223,7 +225,7 @@
         def across(m):
             recv((name, "s", m), span(2))
             for d in (1, -1):
-                p = place(steps[m], -d, 0 if d == 1 else 1)
+                p = place(steps[m], -d, 0 if d == 1 else 1, 16 if m in (1, 2) else 0)
                 send((name, "sf"), name, p, p, secd(d))
 
         def far():
@@ -574,10 +576,10 @@
 
     downs = (WD0, WD1, WD2)
 
-    def partials(p, cc):
+    def partials(p, cc, which):
         mains, ends = [], []
-        for d in order:
-            j = mod4(y + d) * 2 + cc
+        for n in which:
+            j = mod4(y + order[n]) * 2 + cc
             mains.append(downs[p][pl.ds(pl.multiple_of(j * 128, 128), 128), :])
             for k in range(2):
                 at = pl.multiple_of((j * 2 + k) * HW + p * PART, 16)
@@ -591,20 +593,21 @@
     def at_po(p, m):
         return pl.ds(m * OWN + p * 128, 128)
 
-    def give(p):
+    def give(p, which):
         l = pl.ds(p * 128, 128)
-        both = partials(p, o).astype(BF16)
-        for n in range(4):
-            SP[n, :, l] = both[:, n * 128 : (n + 1) * 128]
-            send(("sp", p), "sp", SP.at[n, :, l], RP.at[n, :, l], partner)
-
-    def keep(p):
+        both = partials(p, o, which).astype(BF16)
+        for k, n in enumerate(which):
+            SP[n, :, l] = both[:, k * 128 : (k + 1) * 128]
+            send(("sp", p, which), "sp", SP.at[n, :, l], RP.at[n, :, l], partner)
+
+    def keep(p, which):
         l = pl.ds(p * 128, 128)
-        mine = partials(p, c)
+        mine = partials(p, c, which)
         with scope("sp"):
-            recv(("sp", p), RP.at[:, :, l])
-        for n, d in enumerate(order):
-            both = mine[:, n * 128 : (n + 1) * 128] + RP[n, :, l].astype(F32)
+            recv(("sp", p, which), RP.at[pl.ds(which[0], len(which)), :, l])
+        for k, n in enumerate(which):
+            d = order[n]
+            both = mine[:, k * 128 : (k + 1) * 128] + RP[n, :, l].astype(F32)
             if d == 2:
                 ZS[0, :, l] = both.astype(BF16)
                 send(("rl", p), "rl", ZS.at[0, pl.ds(0, OWN), l], RL.at[0, :, l], at_y(1))
@@ -632,39 +635,42 @@
         return ACC[:, at_po(p, 3)] + RV[0, :, l].astype(F32) + RV[1, :, l].astype(F32)
 
     with scope("give0"):
-        give(0)
+        give(0, EVERY)
     with scope("p6"):
         run(d1, "across", 1)
         run(d2, "relay")
         run(d2, "second", 1)
-        run(d2, "second", 2)
     with scope("keep0"):
-        keep(0)
+        keep(0, EVERY)
     with scope("p7"):
         run(d1, "across", 2)
         run(d1, "across", 3)
+        run(d2, "second", 2)
         run(d2, "across", 0)
         run(d2, "far")
     with scope("p8"):
         run(d2, "across", 1)
         run(d1, "done")
     with scope("give1"):
-        give(1)
+        give(1, EVERY)
     with scope("p8b"):
         run(d2, "across", 2)
         run(d2, "across", 3)
     with scope("pass0"):
         pass_on(0)
     with scope("keep1"):
-        keep(1)
+        keep(1, EVERY)
     with scope("p10"):
         run(d2, "done")
     with scope("give2"):
-        give(2)
+        give(2, FAR)
+        give(2, REST)
+    with scope("keep2"):
+        keep(2, FAR)
     with scope("pass1"):
         pass_on(1)
-    with scope("keep2"):
-        keep(2)
+    with scope("keep2r"):
+        keep(2, REST)
     with scope("pass2"):
         pass_on(2)
     with scope("final0"):

time: 133 us -> 131 us (0.985)
  Pallas kernels: 132 us -> 130 us
    pallas_call x1, Pallas kernels: 132 us -> 130 us  [body(): pl.pallas_call(kernel, out_shape=pltpu.VMEM((TOK, OWN), BF16), in_specs=[...]
where the time goes in v5:
time: 131 us
  Pallas kernels  130 us (99%)
    pallas_call x1, Pallas kernels, body(): pl.pallas_call(kernel, out_shape=pltpu.VMEM((TOK, OWN), BF16), in_specs=[...  130 us

profile of v5, /device:TPU:0, one launch (start us, length us, event | category | flops | bytes accessed | tf_op | source)
XLA Modules:
  0.0 130.9 jit_solution(10362601776520999480)
XLA Ops:
  0.0 130.1 %shard_map.145 = bf16[768,384]{1,0:T(8,128)(2,1)S(1)} custom-call(bf16[192,1056]{1,0:T(8,128)(2,1)} %wg_ref.1, bf16[192,1056]{1,0:T(8,128)(2,1)} %wv_ref.1, bf16[192,1056]{1,0:T(8,128)(2,1)} %bitcast.7, bf16[192,768]{1,0:T(8,128)(2,1)} %bitcast.8, bf16[192,768]{1,0:T(8,128)(2,1)} %bitcast.9, bf16[192,768]{1,0:T(8,128)(2,1)} %bitcast.10, ...), custom_call_target="tpu_custom_call" | custom-call | tf_op jit(solution)/shard_map/pallas_call | solution.py:726
  130.1 0.8 copy.17

commit v6 on v5

--- a/solution.py
+++ b/solution.py
@@ -21,7 +21,7 @@
 EPS = 1e-6
 EVERY, FAR, REST = (0, 1, 2, 3), (0,), (1, 2, 3)
 VLIM = 60
-SEMS = 95
+SEMS = 61
 scope = jax.named_scope
 
 
@@ -154,44 +154,48 @@
     for dev in peers:
         pl.semaphore_signal(barrier, inc=1, device_id=dev, device_id_type=MESH)
 
-    local = []
-
-    def bring(src, dst):
-        d = pltpu.make_async_copy(src, dst, lsem.at[len(local)])
-        d.start()
-        local.append(d)
+    groups = ["main", "tail", "fg", "ig", "seg", "heads", "down", "hg", "gain", "taps", "resid", "wo"]
+
+    def bring(group, src, dst):
+        pltpu.make_async_copy(src, dst, lsem.at[groups.index(group)]).start()
+
+    def landed(group, span):
+        pltpu.make_async_copy(span, span, lsem.at[groups.index(group)]).wait()
 
     own_w = pl.ds(pl.multiple_of(sp * HW, 16), HW)
-    bring(wg_ref.at[:, 0:MAIN], W.at[own_w, 0:MAIN])
-    bring(wv_ref.at[:, 0:MAIN], W.at[own_w, GW:LANES])
+    bring("main", wg_ref.at[:, 0:MAIN], W.at[own_w, 0:MAIN])
+    bring("main", wv_ref.at[:, 0:MAIN], W.at[own_w, GW:LANES])
     for n, ref in enumerate((wg_ref, wv_ref, wd_ref)):
-        bring(ref.at[:, MAIN : MAIN + 32], TL.at[n])
-    bring(fg_hbm, fg_ref)
-    bring(ig_hbm, ig_ref)
-    bring(seg_hbm, seg_ref)
-    bring(k_hbm, KT)
-    bring(v_hbm, VT)
-    bring(q_hbm, QT)
-    bring(og_hbm, OG)
+        bring("tail", ref.at[:, MAIN : MAIN + 32], TL.at[n])
+    bring("fg", fg_hbm, fg_ref)
+    bring("ig", ig_hbm, ig_ref)
+    bring("seg", seg_hbm, seg_ref)
+    bring("heads", k_hbm, KT)
+    bring("heads", v_hbm, VT)
+    bring("heads", q_hbm, QT)
+    bring("heads", og_hbm, OG)
     for n, ref in enumerate((WD0, WD1, WD2)):
         bring(
+            "down",
             wd_ref.at[n * PART : (n + 1) * PART, 0:MAIN],
             ref.at[pl.ds(pl.multiple_of(sp * PART, 16), PART), :],
         )
-    bring(hg_hbm, hg_ref)
-    bring(gain_hbm, gain_ref)
-    bring(taps_hbm, taps_ref)
-    bring(resid_hbm, RB)
+    bring("hg", hg_hbm, hg_ref)
+    bring("gain", gain_hbm, gain_ref)
+    bring("taps", taps_hbm, taps_ref)
+    bring("resid", resid_hbm, RB)
     bring(
+        "wo",
         wo_ref.at[:, pl.ds(pl.multiple_of(tp * OWN, 128), OWN)],
         WO.at[pl.ds(pl.multiple_of(tp * HW, 16), HW), :],
     )
 
-    def stage(name, ref, stride, rows, lanes, by_lanes, first):
+    def stage(gather, ref, stride, rows, lanes, by_lanes, first):
         x_first = first == "x"
         prim = at_x if x_first else at_z
         secd = at_z if x_first else at_x
         steps = (0, -1, 1, 2)
+        group = "gv" if ref is W else "dn"
 
         def place(dp, ds, half=None, shift=0):
             zz, xx = (mod4(z + ds), mod4(x + dp)) if x_first else (mod4(z + dp), mod4(x + ds))
@@ -204,57 +208,58 @@
             row = pl.multiple_of((zz * 4 + xx) * stride + r0, 16)
             return ref.at[pl.ds(row, nr), pl.ds(l0, nl)]
 
-        def span(k):
-            return ref.at[pl.ds(0, k * rows[1]), pl.ds(lanes[0], lanes[1])]
-
         def primary():
             for d in (1, -1):
-                send((name, "p"), name, place(0, 0), place(0, 0), prim(d))
+                send((gather, "p"), group, place(0, 0), place(0, 0), prim(d))
 
         def second(m):
             p = place(steps[m], 0)
             for d in (1, -1):
-                send((name, "s", m), name, p, p, secd(d))
+                send((gather, "s", m), group, p, p, secd(d))
 
         def relay():
-            recv((name, "p"), span(2))
             for d in (1, -1):
                 p = place(-d, 0, 0 if d == 1 else 1)
-                send((name, "pf"), name, p, p, prim(d))
+                send((gather, "pf"), group, p, p, prim(d))
 
         def across(m):
-            recv((name, "s", m), span(2))
             for d in (1, -1):
                 p = place(steps[m], -d, 0 if d == 1 else 1, 16 if m in (1, 2) else 0)
-                send((name, "sf"), name, p, p, secd(d))
+                send((gather, "sf"), group, p, p, secd(d))
 
         def far():
-            recv((name, "pf"), span(1))
             second(3)
 
-        def done():
-            recv((name, "sf"), span(4))
-
-        def out():
-            sent(name, span(15))
-
-        return primary, second, relay, across, far, done, out
-
-    def run(stages, what, *args):
-        k = ("primary", "second", "relay", "across", "far", "done", "out").index(what)
-        for st in stages:
-            st[k](*args)
+        return primary, second, relay, across, far
+
+    awaited = {"relay": ("p", 2), "across": ("s", 2), "far": ("pf", 1), "done": ("sf", 4)}
+
+    def run(gather, what, *args, only=(0, 1)):
+        name, ref, rows, parts = gather
+        if what in awaited:
+            tag, count = awaited[what]
+            recv((name, tag, *args), ref.at[pl.ds(0, count * rows), :])
+        if what != "done":
+            k = ("primary", "second", "relay", "across", "far").index(what)
+            for n in only:
+                parts[n][k](*args)
 
     gv = (
-        stage("g", W, HW, (0, HW), (0, GW), False, "x"),
-        stage("v", W, HW, (0, HW), (GW, MAIN), False, "z"),
+        "gv",
+        W,
+        HW,
+        (
+            stage("gv", W, HW, (0, HW), (0, GW), False, "x"),
+            stage("gv", W, HW, (0, HW), (GW, MAIN), False, "z"),
+        ),
     )
 
     def down_stage(n, ref, cut):
-        return (
-            stage(("da", n), ref, PART, (0, cut), (0, MAIN), True, "x"),
-            stage(("db", n), ref, PART, (cut, PART - cut), (0, MAIN), True, "z"),
+        parts = (
+            stage(n, ref, PART, (0, cut), (0, MAIN), True, "x"),
+            stage(n, ref, PART, (cut, PART - cut), (0, MAIN), True, "z"),
         )
+        return n, ref, PART, parts
 
     d0, d1, d2 = down_stage(0, WD0, 16), down_stage(1, WD1, 32), down_stage(2, WD2, 32)
 
@@ -298,14 +303,13 @@
     mix_g = over_tp("m", mix_block, lambda k: MIX.at[pl.ds(0, k * HW), :])
     x_g = over_tp("x", x_block, lambda k: X.at[:, pl.ds(0, k * OWN)])
 
-    for d in local[:5]:
-        d.wait()
+    landed("main", W.at[0 : 2 * HW, 0:MAIN])
+    landed("tail", TL)
     tails = jnp.concatenate([TL[0], TL[1], TL[2], jnp.zeros((HW, 32), BF16)], axis=1)
     W[own_w, MAIN:GW] = tails
     with scope("barrier"):
         pl.semaphore_wait(barrier, len(peers))
-    run(gv[1:], "primary")
-    run(gv[:1], "primary")
+    run(gv, "primary", only=(1, 0))
     for n in range(1, 8):
         t = lax.rem(tp + n, 8)
         src = wo_ref.at[:, pl.ds(pl.multiple_of(t * OWN, 128), OWN)]
@@ -314,8 +318,9 @@
 
     lane = lax.broadcasted_iota(jnp.int32, (8, TOK), 1)
     row8 = lax.broadcasted_iota(jnp.int32, (8, TOK), 0)
-    for d in local[5:8]:
-        d.wait()
+    landed("fg", fg_ref)
+    landed("ig", ig_ref)
+    landed("seg", seg_ref)
     seg = seg_ref[...].reshape(1, TOK).astype(F32)
     fg = jnp.where(row8 == 0, fg_ref[0:1], fg_ref[1:2])
     e = jnp.exp(-jnp.abs(fg))
@@ -328,8 +333,7 @@
     b = [ig_ref[h : h + 1] - cum[h : h + 1] for h in range(2)]
     end = [cum[h : h + 1, TOK - 1 :] for h in range(2)]
     first, last, second_last = seg[:, :1], seg[:, TOK - 1 :], seg[:, TOK - 2 : TOK - 1]
-    for d in local[8:12]:
-        d.wait()
+    landed("heads", MIX.at[0 : 4 * HW, :])
     ST[...] = jnp.zeros_like(ST)
     peak = []
     for h in range(2):
@@ -383,8 +387,10 @@
         for h in range(2):
             cand[h].append(jnp.where(valid, m[h : h + 1] + dec[h], ABSENT))
             dec[h] = dec[h] + m[2 + h : 3 + h]
-    for d in local[12:18]:
-        d.wait()
+    landed("down", WD0.at[0:HW, :])
+    landed("hg", hg_ref)
+    landed("gain", gain_ref)
+    landed("taps", taps_ref)
     gain_at = lax.broadcasted_iota(jnp.int32, (HW, HW), 0) == lax.broadcasted_iota(jnp.int32, (HW, HW), 1)
     gain_c = jnp.sum(jnp.where(gain_at, hg_ref[...], 0.0), axis=1, keepdims=True)
     for h in range(2):
@@ -422,8 +428,8 @@
     )
     NF[...] = jnp.transpose(jnp.concatenate([flags, jnp.zeros((120, TOK), F32)], axis=0))
     with scope("wo"):
-        for d in local[18:]:
-            d.wait()
+        landed("resid", RB)
+        landed("wo", WO.at[0:HW, :])
         recv("w", WO.at[pl.ds(0, 7 * HW), :])
         WOT[...] = jnp.transpose(WO[...])
 
@@ -549,10 +555,10 @@
         lax.fori_loop(2, 4, value_sum, 0)
     with scope("p4"):
         run(d0, "across", 3)
+        run(d2, "primary")
+        run(d2, "second", 0)
         run(d1, "second", 1)
         run(d1, "second", 2)
-        run(d2, "primary")
-        run(d2, "second", 0)
         run(d1, "across", 0)
     with scope("edge"):
         recv("e", EDGE)
@@ -637,17 +643,17 @@
     with scope("give0"):
         give(0, EVERY)
     with scope("p6"):
-        run(d1, "across", 1)
         run(d2, "relay")
         run(d2, "second", 1)
+        run(d1, "across", 1)
     with scope("keep0"):
         keep(0, EVERY)
     with scope("p7"):
         run(d1, "across", 2)
         run(d1, "across", 3)
         run(d2, "second", 2)
+        run(d2, "far")
         run(d2, "across", 0)
-        run(d2, "far")
     with scope("p8"):
         run(d2, "across", 1)
         run(d1, "done")
@@ -664,9 +670,10 @@
         run(d2, "done")
     with scope("give2"):
         give(2, FAR)
-        give(2, REST)
     with scope("keep2"):
         keep(2, FAR)
+    with scope("give2r"):
+        give(2, REST)
     with scope("pass1"):
         pass_on(1)
     with scope("keep2r"):
@@ -688,8 +695,8 @@
         out_ref[:, 128:256] = (RES[:, 128:256] + jnp.where(low, part2, 0.0)).astype(BF16)
         out_ref[:, 256:384] = (RES[:, 256:384] + jnp.where(low, 0.0, part2)).astype(BF16)
     with scope("sent"):
-        for part in (gv, d0, d1, d2):
-            run(part, "out")
+        sent("gv", W.at[pl.ds(0, 15 * HW), :])
+        sent("dn", W.at[pl.ds(0, 15 * HW), pl.ds(0, MAIN)])
         mix_g[4]()
         x_g[4]()
         sent("w", WO.at[pl.ds(0, 7 * HW), :])
@@ -767,7 +774,7 @@
             pltpu.VMEM((2, OWN, OWN), BF16),
             pltpu.VMEM((2, TOK, OWN), BF16),
             pltpu.SemaphoreType.DMA((SEMS,)),
-            pltpu.SemaphoreType.DMA((20,)),
+            pltpu.SemaphoreType.DMA((12,)),
         ],
         compiler_params=pltpu.CompilerParams(
             collective_id=0, has_side_effects=True, vmem_limit_bytes=VLIM * 1024 * 1024

time: 131 us -> 131 us (level)
  no operation moved by 1% of the time
where the time goes in v6:
time: 131 us; the launch traced here: 130 us
  Pallas kernels  129 us (98%)
    pallas_call x1, Pallas kernels, body(): pl.pallas_call(kernel, out_shape=pltpu.VMEM((TOK, OWN), BF16), in_specs=[...  129 us

profile of v6, /device:TPU:0, one launch (start us, length us, event | category | flops | bytes accessed | tf_op | source)
XLA Modules:
  0.0 130.3 jit_solution(18089296299892752562)
XLA Ops:
  0.0 129.5 %shard_map.145 = bf16[768,384]{1,0:T(8,128)(2,1)S(1)} custom-call(bf16[192,1056]{1,0:T(8,128)(2,1)} %wg_ref.1, bf16[192,1056]{1,0:T(8,128)(2,1)} %wv_ref.1, bf16[192,1056]{1,0:T(8,128)(2,1)} %bitcast.7, bf16[192,768]{1,0:T(8,128)(2,1)} %bitcast.8, bf16[192,768]{1,0:T(8,128)(2,1)} %bitcast.9, bf16[192,768]{1,0:T(8,128)(2,1)} %bitcast.10, ...), custom_call_target="tpu_custom_call" | custom-call | tf_op jit(solution)/shard_map/pallas_call | solution.py:733
  129.5 0.8 copy.17

commit v7 on v6

--- a/solution.py
+++ b/solution.py
@@ -224,7 +224,7 @@
 
         def across(m):
             for d in (1, -1):
-                p = place(steps[m], -d, 0 if d == 1 else 1, 16 if m in (1, 2) else 0)
+                p = place(steps[m], -d, 0 if d == 1 else 1, 16 if m == 1 else 0)
                 send((gather, "sf"), group, p, p, secd(d))
 
         def far():
@@ -334,14 +334,23 @@
     end = [cum[h : h + 1, TOK - 1 :] for h in range(2)]
     first, last, second_last = seg[:, :1], seg[:, TOK - 1 :], seg[:, TOK - 2 : TOK - 1]
     landed("heads", MIX.at[0 : 4 * HW, :])
-    ST[...] = jnp.zeros_like(ST)
-    peak = []
+    peak, made = [], []
     for h in range(2):
         hs = slice(h * DH, h * DH + DH)
         top = jnp.max(jnp.where(seg == last, b[h], ABSENT), axis=1, keepdims=True)
         peak.append(top)
         w = jnp.where(seg == last, jnp.exp(jnp.minimum(b[h] - top, 0.0)), 0.0) * DH**-0.5
-        ST[hs, 0:DH] = dot_t(VT[hs, :], (KT[hs, :].astype(F32) * w).astype(BF16)).astype(BF16)
+        made.append(
+            jnp.concatenate(
+                [dot_t(VT[hs, :], (KT[hs, :].astype(F32) * w).astype(BF16)), jnp.zeros((DH, 32), F32)],
+                axis=1,
+            )
+        )
+    lane96 = lax.broadcasted_iota(jnp.int32, (DH, 128), 1)
+    lane48 = lax.broadcasted_iota(jnp.int32, (48, 128), 1)
+    turned1 = pltpu.roll(made[1], 96, 1)
+    ST[0:DH, :] = jnp.where(lane96 < DH, made[0], turned1).astype(BF16)
+    ST[DH:144, :] = jnp.where(lane48 < 64, turned1[0:48], pltpu.roll(turned1[48:96], 64, 1)).astype(BF16)
     meta_row = lax.broadcasted_iota(jnp.int32, (8, 128), 0)
     meta = jnp.zeros((8, 128), F32)
     for n, value in enumerate((end[0] + peak[0], end[1] + peak[1], end[0], end[1], first, last, second_last)):
@@ -393,15 +402,21 @@
     landed("taps", taps_ref)
     gain_at = lax.broadcasted_iota(jnp.int32, (HW, HW), 0) == lax.broadcasted_iota(jnp.int32, (HW, HW), 1)
     gain_c = jnp.sum(jnp.where(gain_at, hg_ref[...], 0.0), axis=1, keepdims=True)
+    pins = [
+        jnp.maximum(jnp.maximum(p[0], p[1]), jnp.maximum(p[2], p[3])) for p in cand
+    ]
+    upper, lower = jnp.zeros((DH, 128), F32), jnp.zeros((48, 128), F32)
+    for n in range(4):
+        f0, f1 = jnp.exp(cand[0][n] - pins[0]), jnp.exp(cand[1][n] - pins[1])
+        upper = upper + jnp.where(lane96 < DH, f0, f1) * SR[n, 0:DH, :].astype(F32)
+        lower = lower + f1 * SR[n, DH:144, :].astype(F32)
+    lower = jnp.concatenate([lower, pltpu.roll(lower, 64, 1)], axis=0)
+    second_state = jnp.where(lane96 >= DH, upper, jnp.where(lane96 < 64, lower, 0.0))
+    states = [upper, pltpu.roll(second_state, 32, 1)]
     for h in range(2):
         hs = slice(h * DH, h * DH + DH)
-        pin = jnp.maximum(
-            jnp.maximum(cand[h][0], cand[h][1]), jnp.maximum(cand[h][2], cand[h][3])
-        )
-        state = jnp.zeros((DH, 128), F32)
-        for n in range(4):
-            state = state + jnp.exp(cand[h][n] - pin) * SR[n, hs, :].astype(F32)
-        inter = dot(state[:, 0:DH].astype(BF16), QT[hs, :])
+        pin = pins[h]
+        inter = dot(states[h][:, 0:DH].astype(BF16), QT[hs, :])
         m_in = jnp.concatenate(tops[h], axis=1)
         m_pin = jnp.where(seg == first, pin[:, :1], ABSENT)
         m_all = jnp.maximum(m_in, m_pin)
@@ -758,8 +773,8 @@
             pltpu.VMEM((TOK, OWN), BF16),
             pltpu.VMEM((HW, TOK), F32),
             pltpu.VMEM((TOK, 128), F32),
-            pltpu.VMEM((HW, 128), BF16),
-            pltpu.VMEM((4, HW, 128), BF16),
+            pltpu.VMEM((144, 128), BF16),
+            pltpu.VMEM((4, 144, 128), BF16),
             pltpu.VMEM((8, 128), F32),
             pltpu.VMEM((4, 8, 128), F32),
             pltpu.VMEM((8, 8, TOK), F32),

time: 131 us -> 130 us (level)
  no operation moved by 1% of the time
where the time goes in v7:
time: 130 us; the launch traced here: 129 us
  Pallas kernels  128 us (98%)
    pallas_call x1, Pallas kernels, body(): pl.pallas_call(kernel, out_shape=pltpu.VMEM((TOK, OWN), BF16), in_specs=[...  128 us

profile of v7, /device:TPU:0, one launch (start us, length us, event | category | flops | bytes accessed | tf_op | source)
XLA Modules:
  0.0 129.1 jit_solution(8068962558993385061)
XLA Ops:
  0.0 128.3 %shard_map.145 = bf16[768,384]{1,0:T(8,128)(2,1)S(1)} custom-call(bf16[192,1056]{1,0:T(8,128)(2,1)} %wg_ref.1, bf16[192,1056]{1,0:T(8,128)(2,1)} %wv_ref.1, bf16[192,1056]{1,0:T(8,128)(2,1)} %bitcast.7, bf16[192,768]{1,0:T(8,128)(2,1)} %bitcast.8, bf16[192,768]{1,0:T(8,128)(2,1)} %bitcast.9, bf16[192,768]{1,0:T(8,128)(2,1)} %bitcast.10, ...), custom_call_target="tpu_custom_call" | custom-call | tf_op jit(solution)/shard_map/pallas_call | solution.py:748
  128.3 0.8 copy.17
